TPU v7x, 32 devices: a whole 2x2x4 slice. The times are simulated.
32 devices in a mesh: ep: 8 (over z, x), tp: 4 (over y, core).
Axes of the slice: x: 2, y: 2, z: 4, core: 2. Of those that a mesh axis runs over, the one named last changes fastest.
Arguments:
- tokens_first: bfloat16 [4096, 2048], P('ep'), may hold values from -6 to 6
- attn_gain: float32 [2048], replicated, may hold values from 0.1 to 1.9
- w_query: bfloat16 [2048, 1024], P(None, 'tp'), may hold values from -6 to 6
- key_matrix: bfloat16 [2048, 512], P(None, 'tp'), may hold values from -6 to 6
- value_matrix: bfloat16 [2048, 512], P(None, 'tp'), may hold values from -0.125 to 0.125
- head_sink_logit: float32 [16], P('tp'), may hold values from 1 to 5
- w_output: bfloat16 [1024, 2048], P('tp'), may hold values from -0.75 to 0.75
- tokens_second: bfloat16 [1024, 2048], P('ep'), may hold values from -6 to 6
- ffn_gain: float32 [2048], replicated, may hold values from 0.1 to 1.9
- routes: int32 [1024, 4], P('ep'), may hold values from 0 to 15, all different within a row; in each aligned block of 128 rows (0 to 127, 128 to 255, ...) at most 64 rows name the same one
- route_weight: float32 [1024, 4], P('ep'), may hold values from 0.2 to 1.5
- w_gate_exp: bfloat16 [16, 2048, 2048], P('ep', None, 'tp'), may hold values from -0.125 to 0.125
- w_up_exp: bfloat16 [16, 2048, 2048], P('ep', None, 'tp'), may hold values from -0.125 to 0.125
- w_down_exp: bfloat16 [16, 2048, 2048], P('ep', 'tp'), may hold values from -0.125 to 0.125
- w_gate_shared: bfloat16 [2048, 1024], P(None, 'tp'), may hold values from -0.125 to 0.125
- w_up_shared: bfloat16 [2048, 1024], P(None, 'tp'), may hold values from -0.125 to 0.125
- w_down_shared: bfloat16 [1024, 2048], P('tp'), may hold values from -0.1875 to 0.1875
Outputs:
- mixer_out: bfloat16 [4096, 2048], P(('ep', 'tp'))
- moe_out: bfloat16 [1024, 2048], P('ep', 'tp')
Inputs may be any that keep to these rules, and one draw needn't show every extreme that they name: `routes`: each row names 4 different experts; among the rows of one index of ep no expert is named more than 64 times, a bound that some block reaches.
All inputs are finite; a program needn't handle non-finite values.
Results may differ from a plain program's by a relative error of at most 0.017.
Values may be sent and summed in bfloat16 or wider, within the bound.
A program may use at most 64 MiB of HBM per device.

v0:
```python
import functools
import jax
import jax.numpy as jnp
from jax import lax
from jax.experimental import pallas as pl
from jax.experimental.pallas import tpu as pltpu
from jax.sharding import PartitionSpec as P

MODEL_WIDTH = 2048
HEAD_SIZE = 64
BAND_LENGTH = 128


rope_base = 10000.0
norm_eps = 1e-06


def from_behind(value, axis, by):
    devices = lax.axis_size(axis)
    pairs = [(i, i + by) for i in range(devices) if 0 <= i + by < devices]
    return lax.ppermute(value, axis, pairs)


def rms_scale(inputs, gain):
    wide = inputs.astype(jnp.float32)
    scaled = wide * lax.rsqrt(jnp.mean(wide * wide, axis=-1, keepdims=True) + norm_eps)
    return (scaled * gain).astype(jnp.bfloat16)


def apply_rotary(heads, token_positions):
    freqs = rope_base ** (-jnp.arange(0, HEAD_SIZE, 2, dtype=jnp.float32) / HEAD_SIZE)
    angles = token_positions[:, None] * freqs[None, :]
    cosine = jnp.cos(angles)[:, None, :]
    sine = jnp.sin(angles)[:, None, :]
    first_half, second_half = jnp.split(heads, 2, axis=-1)
    return jnp.concatenate(
        [first_half * cosine - second_half * sine, second_half * cosine + first_half * sine],
        axis=-1,
    )


MESH = pl.DeviceIdType.MESH


def whereabouts():
    me, t = lax.axis_index("ep"), lax.axis_index("tp")
    z, x, y, c = me // 2, me % 2, t // 2, t % 2
    zs = (z, z + 1 - 2 * (z % 2), (z + 2) % 4, 3 - z)
    return me, x, y, c, zs


def cols(yy, cc, width):
    return pl.ds(pl.multiple_of((yy * 2 + cc) * width, 128), width)


def rows_of(index, count):
    return pl.ds(pl.multiple_of(index * count, 16), count)


def gather_kernel(
    n_ep, x_ref, meta_ref, halo_ref, out_ref, meta_out, halo_out,
    zs_, zr_, xs_, xr_, ys_, yr_, cs_, cr_, ms_, mr_, hs_, hr_,
):
    me, x, y, c, zs = whereabouts()
    rows, width = x_ref.shape[0], x_ref.shape[1] // 4
    z_peer = [{"ep": zd * 2 + x, "tp": y * 2 + c} for zd in zs]
    x_peer = {"ep": zs[0] * 2 + 1 - x, "tp": y * 2 + c}
    y_peer = {"ep": me, "tp": (1 - y) * 2 + c}
    c_peer = {"ep": me, "tp": y * 2 + 1 - c}
    barrier = pltpu.get_barrier_semaphore()
    for e in range(1, n_ep):
        pl.semaphore_signal(
            barrier, inc=1, device_id={"ep": (me + e) % n_ep, "tp": y * 2 + c}, device_id_type=MESH
        )
    for peer in (y_peer, c_peer):
        pl.semaphore_signal(barrier, inc=1, device_id=peer, device_id_type=MESH)
    pl.semaphore_wait(barrier, n_ep + 1)

    started = []

    def make(blk, yy, peer, send, recv, own=False):
        at = out_ref.at[rows_of(blk, rows), cols(yy, c, width)]
        return pltpu.make_async_remote_copy(
            src_ref=x_ref.at[:, cols(yy, c, width)] if own else at,
            dst_ref=at, send_sem=send, recv_sem=recv, device_id=peer, device_id_type=MESH,
        )

    def go(*a, **k):
        copy = make(*a, **k)
        copy.start()
        started.append(copy)

    for d in (1, 2, 3):
        go(me, y, z_peer[d], zs_.at[d], zr_.at[d], own=True)
        if d == 1:
            go(me, y, x_peer, xs_.at[0], xr_.at[0], own=True)
    go(me, 1 - y, z_peer[1], zs_.at[0], zr_.at[0], own=True)
    go(me, 1 - y, x_peer, xs_.at[4], xr_.at[4], own=True)

    def meta_copy(e, to):
        return pltpu.make_async_remote_copy(
            src_ref=meta_ref, dst_ref=meta_out.at[to], send_sem=ms_.at[e], recv_sem=mr_.at[e],
            device_id={"ep": (me + e) % n_ep, "tp": y * 2 + c}, device_id_type=MESH,
        )

    for e in range(1, n_ep):
        meta_copy(e, me).start()
    halo = pltpu.make_async_remote_copy(
        src_ref=halo_ref, dst_ref=halo_out, send_sem=hs_, recv_sem=hr_,
        device_id={"ep": (me + 1) % n_ep, "tp": y * 2 + c}, device_id_type=MESH,
    )

    @pl.when(me < n_ep - 1)
    def _():
        halo.start()

    @pl.when(me == 0)
    def _():
        halo_out[...] = jnp.zeros_like(halo_out)

    out_ref[rows_of(me, rows), :] = x_ref[...]
    meta_out[me] = meta_ref[...]

    c_list = []

    def arrived(blk, yy, sem, peer):
        make(blk, yy, peer, sem, sem).wait_recv()

    def to_core(blk, yy):
        i = len(c_list)
        c_list.append((blk, yy))
        go(blk, yy, c_peer, cs_.at[i], cr_.at[i])

    y_list = []

    def to_y(blk):
        i = len(y_list)
        y_list.append(blk)
        go(blk, y, y_peer, ys_.at[i], yr_.at[i])

    def blk(d, xx):
        return zs[d] * 2 + xx

    for d in (1, 2, 3):
        arrived(blk(d, x), y, zr_.at[d], c_peer)
        go(blk(d, x), y, x_peer, xs_.at[d], xr_.at[d])
        if d != 1:
            to_y(blk(d, x))
        to_core(blk(d, x), y)
        if d == 1:
            arrived(blk(0, 1 - x), y, xr_.at[0], c_peer)
            to_core(blk(0, 1 - x), y)
        if d == 2:
            arrived(blk(0, 1 - x), 1 - y, xr_.at[4], c_peer)
            to_core(blk(0, 1 - x), 1 - y)
    arrived(blk(1, x), 1 - y, zr_.at[0], c_peer)
    to_core(blk(1, x), 1 - y)
    for d in (1, 2, 3):
        arrived(blk(d, 1 - x), y, xr_.at[d], c_peer)
        to_y(blk(d, 1 - x))
        to_core(blk(d, 1 - x), y)
    for i, b in enumerate(list(y_list)):
        arrived(b, 1 - y, yr_.at[i], c_peer)
        to_core(b, 1 - y)
    for i, (b, yy) in enumerate(c_list):
        at = out_ref.at[rows_of(b, rows), cols(yy, 1 - c, width)]
        pltpu.make_async_remote_copy(
            src_ref=at, dst_ref=at, send_sem=cs_.at[i], recv_sem=cr_.at[i],
            device_id=c_peer, device_id_type=MESH,
        ).wait_recv()
    for e in range(1, n_ep):
        meta_copy(e, (me + n_ep - e) % n_ep).wait_recv()

    @pl.when(me > 0)
    def _():
        halo.wait_recv()

    @pl.when(me < n_ep - 1)
    def _():
        halo.wait_send()

    for copy in started:
        copy.wait_send()
    for e in range(1, n_ep):
        meta_copy(e, me).wait_send()


def gather(x, meta, halo, n_ep):
    rows, wide = x.shape
    dma = pltpu.SemaphoreType.DMA
    vm = pl.BlockSpec(memory_space=pltpu.VMEM)
    return pl.pallas_call(
        functools.partial(gather_kernel, n_ep),
        out_shape=(
            jax.ShapeDtypeStruct((n_ep * rows, wide), x.dtype),
            jax.ShapeDtypeStruct((n_ep,) + meta.shape, meta.dtype),
            jax.ShapeDtypeStruct(halo.shape, halo.dtype),
        ),
        in_specs=[vm] * 3,
        out_specs=(vm, vm, vm),
        scratch_shapes=[
            dma((4,)), dma((4,)), dma((5,)), dma((5,)), dma((5,)), dma((5,)),
            dma((14,)), dma((14,)), dma((n_ep,)), dma((n_ep,)), dma, dma,
        ],
        compiler_params=pltpu.CompilerParams(
            collective_id=0, has_side_effects=True, vmem_limit_bytes=40 * 1024 * 1024
        ),
        name="gather_rows",
    )(x, meta, halo)


def ffn_kernel(
    cap, x_ref, meta_ref, wg_ref, wu_ref, wd_ref, sg_ref, su_ref, sd_ref, out_ref, xs, ys
):
    w_count = ys.shape[1] // cap
    j = pl.program_id(0)
    exp_dev = pl.num_programs(0)
    me = lax.axis_index("ep")
    n_ep, _, rows = meta_ref.shape
    topk = meta_ref.shape[1] // 2
    f32 = jnp.float32
    before = (
        lax.broadcasted_iota(jnp.int32, (rows, rows), 0)
        < lax.broadcasted_iota(jnp.int32, (rows, rows), 1)
    ).astype(f32).astype(jnp.bfloat16)

    def placed(s, jj, weighted):
        e = (me * exp_dev + jj).astype(f32)
        named = meta_ref[s, 0:topk, :] == e
        hit = jnp.sum(named.astype(f32), axis=0, keepdims=True)
        rank = jnp.dot(
            jnp.broadcast_to(hit, (16, rows)).astype(jnp.bfloat16), before,
            preferred_element_type=f32,
        )[0:1]
        slot = lax.broadcasted_iota(jnp.int32, (cap, rows), 0).astype(f32)
        value = hit
        if weighted:
            value = jnp.sum(
                jnp.where(named, meta_ref[s, topk : 2 * topk, :], 0.0), axis=0, keepdims=True
            )
        return jnp.where((slot == rank) & (hit > 0.0), value, 0.0)

    for s in range(n_ep):
        xs[pl.ds(s * cap, cap), :] = jnp.dot(
            placed(s, j, False).astype(jnp.bfloat16), x_ref[pl.ds(s * rows, rows), :],
            preferred_element_type=f32,
        ).astype(jnp.bfloat16)
    rows_in = xs[...]
    gate = jnp.dot(rows_in, wg_ref[0], preferred_element_type=f32)
    up = jnp.dot(rows_in, wu_ref[0], preferred_element_type=f32)
    hidden = (gate / (1.0 + jnp.exp(-gate)) * up).astype(jnp.bfloat16)
    res = jnp.dot(hidden, wd_ref[0], preferred_element_type=f32).astype(jnp.bfloat16)
    for s in range(n_ep):
        ys[s, pl.ds(pl.multiple_of(j * cap, cap), cap), :] = res[s * cap : (s + 1) * cap]

    @pl.when(j == exp_dev - 1)
    def _():
        for s in range(n_ep):
            mix = jnp.concatenate([placed(s, jj, True) for jj in range(w_count)], axis=0)
            out_ref[pl.ds(s * rows, rows), :] = jnp.dot(
                mix.T.astype(jnp.bfloat16), ys[s], preferred_element_type=f32
            ).astype(jnp.bfloat16)
        mine = rows_of(me, rows)
        own = x_ref[mine, :]
        sg = jnp.dot(own, sg_ref[...], preferred_element_type=f32)
        su = jnp.dot(own, su_ref[...], preferred_element_type=f32)
        sh = (sg / (1.0 + jnp.exp(-sg)) * su).astype(jnp.bfloat16)
        out_ref[mine, :] = (
            out_ref[mine, :].astype(f32) + jnp.dot(sh, sd_ref[...], preferred_element_type=f32)
        ).astype(jnp.bfloat16)


def experts_of(x, meta, wg, wu, wd, sg, su, sd, cap):
    n_ep, _, rows = meta.shape
    exp_dev, wide, hid = wg.shape
    vm = pl.BlockSpec(memory_space=pltpu.VMEM)
    return pl.pallas_call(
        functools.partial(ffn_kernel, cap),
        grid=(exp_dev,),
        out_shape=jax.ShapeDtypeStruct(x.shape, jnp.bfloat16),
        in_specs=[
            vm, vm,
            pl.BlockSpec((1, wide, hid), lambda j: (j, 0, 0)),
            pl.BlockSpec((1, wide, hid), lambda j: (j, 0, 0)),
            pl.BlockSpec((1, hid, wide), lambda j: (j, 0, 0)),
            vm, vm, vm,
        ],
        out_specs=vm,
        scratch_shapes=[
            pltpu.VMEM((n_ep * cap, wide), jnp.bfloat16),
            pltpu.VMEM((n_ep, exp_dev * cap, wide), jnp.bfloat16),
        ],
        compiler_params=pltpu.CompilerParams(
            dimension_semantics=("arbitrary",), vmem_limit_bytes=58 * 1024 * 1024
        ),
        name="experts",
    )(x, meta, wg, wu, wd, sg, su, sd)


def reduce_kernel(
    moe_ref, mix_ref, moe_out, mix_out, rc, s1, rx, s2, keep, ry, s3, rz, mrc, ms, mry,
    cs_, cr_, xs_, xr_, ys_, yr_, zs_, zr_, ms_, mr_,
):
    me, x, y, c, zs = whereabouts()
    rows, width = moe_out.shape
    mrows = mix_out.shape[0]
    f32 = jnp.float32
    x_peer = {"ep": zs[0] * 2 + 1 - x, "tp": y * 2 + c}
    y_peer = {"ep": me, "tp": (1 - y) * 2 + c}
    c_peer = {"ep": me, "tp": y * 2 + 1 - c}
    z_peer = [{"ep": zd * 2 + x, "tp": y * 2 + c} for zd in zs]
    barrier = pltpu.get_barrier_semaphore()
    for peer in [x_peer, y_peer, c_peer] + z_peer[1:]:
        pl.semaphore_signal(barrier, inc=1, device_id=peer, device_id_type=MESH)
    pl.semaphore_wait(barrier, 6)
    started = []

    def copy(src, dst, peer, send, recv):
        return pltpu.make_async_remote_copy(
            src_ref=src, dst_ref=dst, send_sem=send, recv_sem=recv,
            device_id=peer, device_id_type=MESH,
        )

    def go(*a):
        k = copy(*a)
        k.start()
        started.append(k)

    def got(dst, recv):
        copy(dst, dst, c_peer, recv, recv).wait_recv()

    ysel = (1 - y, y)
    order = (2, 3, 1, 0)

    def mine(d, xx, yy, cc):
        return (rows_of(zs[d] * 2 + xx, rows), cols(yy, cc, width))

    def mixer_core(k):
        go(
            mix_ref.at[rows_of(ysel[k] * 2 + 1 - c, mrows), :], mrc.at[k], c_peer,
            ms_.at[k], mr_.at[k],
        )

    def core(d, col, k):
        i = d * 4 + col * 2 + k
        xx = (1 - x, x)[col]
        at = mine(d, xx, ysel[k], 1 - c)
        go(moe_ref.at[at[0], at[1]], rc.at[i], c_peer, cs_.at[i], cr_.at[i])

    core(order[0], 0, 0)
    core(order[0], 0, 1)
    mixer_core(0)
    for d in order[1:]:
        core(d, 0, 0)
        core(d, 0, 1)
    for d in order:
        core(d, 1, 0)
        core(d, 1, 1)
    mixer_core(1)

    def pair(d, col, k):
        i = d * 4 + col * 2 + k
        xx = (1 - x, x)[col]
        at = mine(d, xx, ysel[k], c)
        got(rc.at[i], cr_.at[i])
        return moe_ref[at[0], at[1]].astype(f32) + rc[i].astype(f32)

    def x_send(d):
        for k in (0, 1):
            i = d * 2 + k
            s1[i] = pair(d, 0, k).astype(jnp.bfloat16)
            go(s1.at[i], rx.at[i], x_peer, xs_.at[i], xr_.at[i])

    x_send(order[0])
    got(mrc.at[0], mr_.at[0])
    ms[...] = (
        mix_ref[rows_of(ysel[0] * 2 + c, mrows), :].astype(f32) + mrc[0].astype(f32)
    ).astype(jnp.bfloat16)
    go(ms, mry, y_peer, ms_.at[2], mr_.at[2])
    for d in order[1:]:
        x_send(d)
    for d in order:
        for k in (0, 1):
            i = d * 2 + k
            part = pair(d, 1, k)
            got(rx.at[i], xr_.at[i])
            part = part + rx[i].astype(f32)
            if k == 0:
                s2[d] = part.astype(jnp.bfloat16)
                go(s2.at[d], ry.at[d], y_peer, ys_.at[d], yr_.at[d])
            else:
                keep[d] = part
    for d in order[:3]:
        got(ry.at[d], yr_.at[d])
        s3[d] = (keep[d] + ry[d].astype(f32)).astype(jnp.bfloat16)
        go(s3.at[d], rz.at[d], z_peer[d], zs_.at[d], zr_.at[d])
    got(mrc.at[1], mr_.at[1])
    got(mry, mr_.at[2])
    mix_out[...] = (
        mix_ref[rows_of(ysel[1] * 2 + c, mrows), :].astype(f32)
        + mrc[1].astype(f32)
        + mry[...].astype(f32)
    ).astype(jnp.bfloat16)
    got(ry.at[0], yr_.at[0])
    total = keep[0] + ry[0].astype(f32)
    for d in order[:3]:
        got(rz.at[d], zr_.at[d])
        total = total + rz[d].astype(f32)
    moe_out[...] = total.astype(jnp.bfloat16)
    for k in started:
        k.wait_send()


def reduce_both(moe, mix, n_ep):
    rows, width = moe.shape[0] // n_ep, moe.shape[1] // 4
    mrows, wide = mix.shape[0] // 4, mix.shape[1]
    dma = pltpu.SemaphoreType.DMA
    vm = pl.BlockSpec(memory_space=pltpu.VMEM)
    bf = jnp.bfloat16
    return pl.pallas_call(
        reduce_kernel,
        out_shape=(
            jax.ShapeDtypeStruct((rows, width), bf),
            jax.ShapeDtypeStruct((mrows, wide), bf),
        ),
        in_specs=[vm, vm],
        out_specs=(vm, vm),
        scratch_shapes=[
            pltpu.VMEM((16, rows, width), bf),
            pltpu.VMEM((8, rows, width), bf),
            pltpu.VMEM((8, rows, width), bf),
            pltpu.VMEM((4, rows, width), bf),
            pltpu.VMEM((4, rows, width), jnp.float32),
            pltpu.VMEM((4, rows, width), bf),
            pltpu.VMEM((4, rows, width), bf),
            pltpu.VMEM((4, rows, width), bf),
            pltpu.VMEM((2, mrows, wide), bf),
            pltpu.VMEM((mrows, wide), bf),
            pltpu.VMEM((mrows, wide), bf),
            dma((16,)), dma((16,)), dma((8,)), dma((8,)), dma((4,)), dma((4,)),
            dma((4,)), dma((4,)), dma((3,)), dma((3,)),
        ],
        compiler_params=pltpu.CompilerParams(
            collective_id=1, has_side_effects=True, vmem_limit_bytes=40 * 1024 * 1024
        ),
        name="reduce_both",
    )(moe, mix)


def local(
    tokens_first,
    attn_gain,
    w_query,
    key_matrix,
    value_matrix,
    head_sink_logit,
    w_output,
    tokens_second,
    ffn_gain,
    routes,
    route_weight,
    w_gate_exp,
    w_up_exp,
    w_down_exp,
    w_gate_shared,
    w_up_shared,
    w_down_shared,
):
    rows_first = tokens_first.shape[0]
    norm_input = rms_scale(tokens_first, attn_gain)
    offset = lax.axis_index("ep") * rows_first
    token_positions = (offset + jnp.arange(rows_first, dtype=jnp.int32)).astype(jnp.float32)
    head_count = w_query.shape[1] // HEAD_SIZE
    key_heads = key_matrix.shape[1] // HEAD_SIZE
    head_group = head_count // key_heads
    query_rows = apply_rotary(
        jnp.dot(norm_input, w_query, preferred_element_type=jnp.float32).reshape(
            rows_first, head_count, HEAD_SIZE
        ),
        token_positions,
    ).astype(jnp.bfloat16)
    keys_local = apply_rotary(
        jnp.dot(norm_input, key_matrix, preferred_element_type=jnp.float32).reshape(
            rows_first, key_heads, HEAD_SIZE
        ),
        token_positions,
    ).astype(jnp.bfloat16)
    values_local = (
        jnp.dot(norm_input, value_matrix, preferred_element_type=jnp.float32)
        .astype(jnp.bfloat16)
        .reshape(rows_first, key_heads, HEAD_SIZE)
    )
    kernels = lax.axis_size("ep") == 8 and lax.axis_size("tp") == 4
    if kernels:
        normed_second = rms_scale(tokens_second, ffn_gain)
        meta = jnp.concatenate([routes.astype(jnp.float32), route_weight], axis=1).T
        halo = jnp.concatenate(
            [
                keys_local[rows_first - BAND_LENGTH :].reshape(BAND_LENGTH, -1),
                values_local[rows_first - BAND_LENGTH :].reshape(BAND_LENGTH, -1),
            ],
            axis=1,
        )
        gathered, metas, before = gather(normed_second, meta, halo, lax.axis_size("ep"))
        split = key_heads * HEAD_SIZE
        keys_before = before[:, :split].reshape(BAND_LENGTH, key_heads, HEAD_SIZE)
        values_before = before[:, split:].reshape(BAND_LENGTH, key_heads, HEAD_SIZE)
    else:
        keys_before, values_before = from_behind(
            (keys_local[rows_first - BAND_LENGTH :], values_local[rows_first - BAND_LENGTH :]),
            "ep",
            1,
        )
    keys_all = jnp.concatenate([keys_before, keys_local], axis=0)
    values_all = jnp.concatenate([values_before, values_local], axis=0)
    band = BAND_LENGTH
    bands = rows_first // band

    def windows(padded):
        return jnp.concatenate(
            [
                padded[:rows_first].reshape(bands, band, key_heads, HEAD_SIZE),
                padded[band:].reshape(bands, band, key_heads, HEAD_SIZE),
            ],
            axis=1,
        )

    sink_scores = head_sink_logit.reshape(key_heads, head_group)[None, :, :, None, None]
    scores = jnp.einsum(
        "bqhgd,bkhd->bhgqk",
        query_rows.reshape(bands, band, key_heads, head_group, HEAD_SIZE),
        windows(keys_all),
        preferred_element_type=jnp.float32,
    ) * HEAD_SIZE ** (-0.5)
    offsets = (
        band
        + jnp.arange(band, dtype=jnp.int32)[:, None]
        - jnp.arange(2 * band, dtype=jnp.int32)[None, :]
    )
    key_pos = (
        offset
        + (jnp.arange(bands, dtype=jnp.int32)[:, None] - 1) * band
        + jnp.arange(2 * band, dtype=jnp.int32)[None, :]
    )
    visible = ((offsets >= 0) & (offsets < band))[None] & (key_pos >= 0)[:, None, :]
    scores = jnp.where(visible[:, None, None], scores, -jnp.inf)
    peak = jnp.maximum(jnp.max(scores, axis=-1, keepdims=True), sink_scores)
    expo = jnp.exp(scores - peak)
    total = jnp.sum(expo, axis=-1, keepdims=True) + jnp.exp(sink_scores - peak)
    weights = (expo / total).astype(jnp.bfloat16)
    attended = (
        jnp.einsum(
            "bhgqk,bkhd->bqhgd", weights, windows(values_all), preferred_element_type=jnp.float32
        )
        .astype(jnp.bfloat16)
        .reshape(rows_first, head_count * HEAD_SIZE)
    )
    if kernels:
        capacity = max(2, 2 * tokens_second.shape[0] * routes.shape[1] // (w_gate_exp.shape[0] * 8))
        mixer_part = jnp.dot(attended, w_output, preferred_element_type=jnp.float32).astype(
            jnp.bfloat16
        )
        moe_part = experts_of(
            gathered, metas, w_gate_exp, w_up_exp, w_down_exp,
            w_gate_shared, w_up_shared, w_down_shared, capacity,
        )
        moe_out, mixer_out = reduce_both(moe_part, mixer_part, lax.axis_size("ep"))
        return (mixer_out, moe_out)
    mixer_out = lax.psum_scatter(
        jnp.dot(attended, w_output, preferred_element_type=jnp.float32).astype(jnp.bfloat16),
        "tp",
        scatter_dimension=0,
        tiled=True,
    )
    rows_second = tokens_second.shape[0]
    topk = routes.shape[1]
    exp_dev = w_gate_exp.shape[0]
    n_expdev = lax.axis_size("ep")
    experts = exp_dev * n_expdev
    capacity = max(2, 2 * rows_second * topk // experts)
    slot_count = experts * capacity
    normed_second = rms_scale(tokens_second, ffn_gain)
    flat = routes.reshape(-1)
    onehot = (flat[:, None] == jnp.arange(experts, dtype=jnp.int32)[None, :]).astype(jnp.int32)
    ranks = jnp.sum((jnp.cumsum(onehot, axis=0) - onehot) * onehot, axis=1)
    slots = flat * capacity + ranks
    match = (jnp.arange(slot_count, dtype=jnp.int32)[:, None] == slots[None, :]).reshape(
        slot_count, rows_second, topk
    )
    dispatch = jnp.sum(match.astype(jnp.float32), axis=2).astype(jnp.bfloat16)
    combine = jnp.sum(match.astype(jnp.float32) * route_weight[None, :, :], axis=2)
    width = normed_second.shape[1] // lax.axis_size("tp")
    feature_slice = lax.dynamic_slice_in_dim(normed_second, lax.axis_index("tp") * width, width, 1)
    outgoing = jnp.dot(dispatch, feature_slice, preferred_element_type=jnp.float32).astype(
        jnp.bfloat16
    )
    arrived = lax.all_to_all(outgoing, "ep", split_axis=0, concat_axis=0, tiled=True)
    piece = lax.all_gather(arrived, "tp", axis=1, tiled=True)
    cols = piece.shape[1]
    part = piece.reshape(n_expdev, exp_dev, capacity, cols)
    gate_pre = jnp.einsum("sjcd,jdf->sjcf", part, w_gate_exp, preferred_element_type=jnp.float32)
    up_pre = jnp.einsum("sjcd,jdf->sjcf", part, w_up_exp, preferred_element_type=jnp.float32)
    hidden = (jax.nn.silu(gate_pre) * up_pre).astype(jnp.bfloat16)
    shared_hidden = (
        jax.nn.silu(jnp.dot(normed_second, w_gate_shared, preferred_element_type=jnp.float32))
        * jnp.dot(normed_second, w_up_shared, preferred_element_type=jnp.float32)
    ).astype(jnp.bfloat16)
    routed_term = jnp.einsum(
        "sjcf,jfd->dsjc", hidden, w_down_exp, preferred_element_type=jnp.float32
    ).reshape(lax.axis_size("tp") * (MODEL_WIDTH // lax.axis_size("tp")), slot_count)
    shared_term = lax.dot_general(
        w_down_shared, shared_hidden, (((0,), (1,)), ((), ())), preferred_element_type=jnp.float32
    )
    summed = lax.psum_scatter(
        jnp.concatenate([routed_term, shared_term], axis=1).astype(jnp.bfloat16),
        "tp",
        scatter_dimension=0,
        tiled=True,
    ).astype(jnp.float32)
    routed_part = summed[:, :slot_count].astype(jnp.bfloat16)
    returned = lax.all_to_all(routed_part, "ep", split_axis=1, concat_axis=1, tiled=True)
    weighted = lax.dot_general(
        combine,
        returned.astype(jnp.float32),
        (((0,), (1,)), ((), ())),
        precision=lax.Precision.HIGHEST,
    )
    moe_out = (weighted + summed[:, slot_count:].T).astype(jnp.bfloat16)
    return (mixer_out, moe_out)


def solution(mesh):
    in_specs = (
        P("ep", None),
        P(),
        P(None, "tp"),
        P(None, "tp"),
        P(None, "tp"),
        P("tp"),
        P("tp", None),
        P("ep", None),
        P(),
        P("ep", None),
        P("ep", None),
        P("ep", None, "tp"),
        P("ep", None, "tp"),
        P("ep", "tp", None),
        P(None, "tp"),
        P(None, "tp"),
        P("tp", None),
    )
    out_specs = (P(("ep", "tp"), None), P("ep", "tp"))
    return jax.shard_map(local, mesh=mesh, in_specs=in_specs, out_specs=out_specs, check_vma=False)
```

profile of v0, /device:TPU:0, one launch (start us, length us, event | category | flops | bytes accessed | tf_op | source)
XLA Modules:
  0.0 116.5 jit_solution(12777972605247823127)
XLA Ops:
  0.7 1.4 %fusion.5 = f32[128]{0:T(128)S(1)} fusion(bf16[128,2048]{1,0:T(8,128)(2,1)} %param.24), kind=kLoop, calls=%fused_computation.15 | loop fusion | flops 786304 | bytes 524800 | tf_op jit(solution)/shard_map/reduce_sum | solution.py:26
  2.1 1.2 %fusion.7.x_ref = bf16[128,2048]{1,0:T(8,128)(2,1)S(1)} fusion(bf16[128,2048]{1,0:T(8,128)(2,1)} %param.24, f32[2048]{0:T(1024)} %param.25, f32[128]{0:T(128)S(1)} %add_rsqrt_fusion.1), kind=kLoop, calls=%fused_computation.17 | loop fusion | flops 1048576 | bytes 1057280 | tf_op jit(solution)/shard_map/convert_element_type | solution.py:27
  3.3 0.7 convert_element_type.43
  4.0 0.7 maximum_bitcast_fusion.4.meta_ref
  4.7 2.1 %fusion = f32[512]{0:T(512)S(1)} fusion(bf16[512,2048]{1,0:T(8,128)(2,1)} %param.17), kind=kLoop, calls=%fused_computation.2 | loop fusion | flops 3145216 | bytes 2099200 | tf_op jit(solution)/shard_map/reduce_sum | solution.py:26
  6.8 0.8 convolution_convert_fusion.2
  7.6 0.2 copy-done.8
  7.8 0.9 fusion.29
  8.8 0.3 multiply_cosine_fusion
  9.2 0.1 copy.27
  9.3 32.5 %gather_rows.1 = (bf16[1024,2048]{1,0:T(8,128)(2,1)S(1)}, f32[8,8,128]{2,1,0:T(8,128)S(1)}, bf16[128,256]{1,0:T(8,128)(2,1)S(1)}) custom-call(bf16[128,2048]{1,0:T(8,128)(2,1)S(1)} %fusion.7.x_ref, f32[8,128]{1,0:T(8,128)S(1)} %maximum_bitcast_fusion.4.meta_ref, bf16[128,256]{1,0:T(8,128)(2,1)S(1)} %pad_maximum_fusion.3.halo_ref), custom_call_target="tpu_custom_call" | custom-call | tf_op jit(solution)/shard_map/gather_rows/pallas_call | solution.py:192
  41.9 2.0 %copy-done.2 = bf16[1024,2048]{1,0:T(8,128)(2,1)} copy-done((bf16[1024,2048]{1,0:T(8,128)(2,1)}, bf16[1024,2048]{1,0:T(8,128)(2,1)S(1)}, u32[]{:S(2)}) %copy-start.2) | copy-done | bytes 4194328
  43.8 0.6 copy-done.3
  44.5 21.4 %experts.1.moe_ref = bf16[1024,2048]{1,0:T(8,128)(2,1)} custom-call(bf16[1024,2048]{1,0:T(8,128)(2,1)} %copy-done.2, f32[8,8,128]{2,1,0:T(8,128)} %copy-done.3, bf16[2,2048,512]{2,1,0:T(8,128)(2,1)} %wg_ref.1, bf16[2,2048,512]{2,1,0:T(8,128)(2,1)} %wu_ref.1, bf16[2,512,2048]{2,1,0:T(8,128)(2,1)} %wd_ref.1, bf16[2048,256]{1,0:T(8,128)(2,1)} %sg_ref.1, ...), custom_call_target="tpu_custom_call" | custom-call | tf_op jit(solution)/shard_map/experts/pallas_call | solution.py:277
  65.9 1.0 fusion.26
  67.1 0.7 copy_bitcast_fusion.2
  67.7 0.6 fusion.31
  68.3 0.1 copy.33
  68.6 0.2 broadcast_and_fusion
  68.8 1.4 %fusion.32 = (f32[4,2,2,128]{3,2,1,0:T(2,128)S(1)}, f32[4,2,2,128,256]{3,4,2,1,0:T(8,128)S(1)}) fusion(bf16[4,128,2,2,32]{1,4,3,2,0:T(8,128)(2,1)S(1)} %copy.38, bf16[4,128,2,2,32]{1,4,3,2,0:T(8,128)(2,1)S(1)} %copy.37, bf16[4,128,2,32]{1,3,2,0:T(8,128)(2,1)} %get-tuple-element.22, bf16[4,128,2,32]{1,3,2,0:T(8,128)(2,1)} %get-tuple-element.23, ...), kind=kOutput, calls=%fused_computation.68 | convolution fusion | flops 69990400 | bytes 2760704 | tf_op jit(solution)/shard_map/bqhgd,bkhd->bhgqk/dot_general | solution.py:529
  70.4 0.3 fusion.3
  70.7 0.7 exponential_add_fusion
  71.4 0.1 reshape.204
  71.5 0.8 copy.32
  72.3 0.1 copy.29
  72.4 0.9 copy.28
  73.4 1.5 %fusion.4 = bf16[4,128,2,2,64]{1,4,3,2,0:T(8,128)(2,1)S(1)} fusion(f32[4,2,2,128,256]{3,4,2,1,0:T(8,128)S(1)} %get-tuple-element.21, f32[4,2,2,128]{3,2,1,0:T(2,128)} %exponential_add_fusion, f32[4,2,2,128]{3,2,1,0:T(2,128)S(1)} %broadcast_maximum_fusion, bf16[4,128,2,64]{1,3,2,0:T(8,128)(2,1)} %copy.32, bf16[4,128,2,64]{1,3,2,0:T(8,128)(2,1)S(1)} %copy_bitcast_fusion.1), kind=kOutput, calls=%fused_computation.13 | convolution fusion | flops 69337088 | bytes 2637824 | tf_op jit(solution)/shard_map/bhgqk,bkhd->bqhgd/dot_general | solution.py:552
  74.9 0.2 copy.40
  75.1 0.7 convolution_convert_fusion.mix_ref
  75.9 39.2 %reduce_both.1 = (bf16[128,512]{1,0:T(8,128)(2,1)S(1)}, bf16[128,2048]{1,0:T(8,128)(2,1)S(1)}) custom-call(bf16[1024,2048]{1,0:T(8,128)(2,1)S(1)} %copy-done.1, bf16[512,2048]{1,0:T(8,128)(2,1)S(1)} %convolution_convert_fusion.mix_ref), custom_call_target="tpu_custom_call" | custom-call | tf_op jit(solution)/shard_map/reduce_both/pallas_call | solution.py:420
  115.1 0.8 copy.62
  115.8 0.7 copy.63
  (40 shorter events, 0.7 us)
Async XLA Ops:
  0.6 74.5 %copy-start = (bf16[256,2048]{1,0:T(8,128)(2,1)S(1)}, bf16[256,2048]{1,0:T(8,128)(2,1)}, u32[]{:S(2)}) copy-start(bf16[256,2048]{1,0:T(8,128)(2,1)} %param.23) | copy-start | bytes 3145732
  0.6 6.1 %copy-start.7 = (bf16[2048,128]{1,0:T(8,128)(2,1)S(1)}, bf16[2048,128]{1,0:T(8,128)(2,1)}, u32[]{:S(2)}) copy-start(bf16[2048,128]{1,0:T(8,128)(2,1)} %param.21) | copy-start | bytes 1572868
  0.7 6.1 %copy-start.4 = (bf16[512,2048]{1,0:T(8,128)(2,1)S(1)}, bf16[512,2048]{1,0:T(8,128)(2,1)}, u32[]{:S(2)}) copy-start(bf16[512,2048]{1,0:T(8,128)(2,1)} %param.17) | copy-start | bytes 6291460
  0.7 6.1 %copy-start.9 = (f32[2048]{0:T(1024)S(1)}, f32[2048]{0:T(1024)}, u32[]{:S(2)}) copy-start(f32[2048]{0:T(1024)} %param.18) | copy-start | bytes 24580
  6.8 1.0 copy-start.8
  41.8 2.0 %copy-start.2 = (bf16[1024,2048]{1,0:T(8,128)(2,1)}, bf16[1024,2048]{1,0:T(8,128)(2,1)S(1)}, u32[]{:S(2)}) copy-start(bf16[1024,2048]{1,0:T(8,128)(2,1)S(1)} %get-tuple-element.7.x_ref) | copy-start | bytes 12582916
  43.8 0.6 copy-start.3
  44.4 21.4 %copy-start.5 = (bf16[512,2048]{1,0:T(8,128)(2,1)S(1)}, bf16[512,2048]{1,0:T(8,128)(2,1)}, u32[]{:S(2)}) copy-start(bf16[512,2048]{1,0:T(8,128)(2,1)} %param.17) | copy-start | bytes 6291460
  44.4 21.4 %copy-start.6 = (bf16[2048,256]{1,0:T(8,128)(2,1)S(1)}, bf16[2048,256]{1,0:T(8,128)(2,1)}, u32[]{:S(2)}) copy-start(bf16[2048,256]{1,0:T(8,128)(2,1)} %param.19) | copy-start | bytes 3145732
  67.0 3.2 %copy-start.10 = (f32[4]{0:T(128)S(1)}, f32[4]{0:T(128)}, u32[]{:S(2)}) copy-start(f32[4]{0:T(128)} %param.22) | copy-start | bytes 52
  73.3 2.5 %copy-start.1 = (bf16[1024,2048]{1,0:T(8,128)(2,1)S(1)}, bf16[1024,2048]{1,0:T(8,128)(2,1)}, u32[]{:S(2)}) copy-start(bf16[1024,2048]{1,0:T(8,128)(2,1)} %experts.1.moe_ref) | copy-start | bytes 12582916
where the time goes:
time: 117 us
  Pallas kernels  93.1 us (80%)
  local copies, waits for them, and re-layouts  8.14 us (7%)
  other arithmetic  8 us (7%)
  matrix products  6.33 us (5%)
    pallas_call x1, Pallas kernels, reduce_both(): pl.pallas_call(reduce_kernel, out_shape=(jax.ShapeDtypeStruct((rows, widt...  39.2 us
    pallas_call x1, Pallas kernels, gather(): pl.pallas_call(functools.partial(gather_kernel, n_ep), out_shape=(jax.Sha...  32.5 us
    pallas_call x1, Pallas kernels, experts_of(): pl.pallas_call(functools.partial(ffn_kernel, cap), grid=(exp_dev,), out_s...  21.4 us
    unnamed x24, local copies, waits for them, and re-layouts  4.33 us
    reduce_sum x2, other arithmetic, rms_scale(): jnp.mean(wide * wide, axis=-1, keepdims=True) + norm_eps  3.45 us

commit v1 on v0

v1 whole, which is shorter than its diff:
```python
import functools
import jax
import jax.numpy as jnp
import numpy as np
from jax import lax
from jax.experimental import pallas as pl
from jax.experimental.pallas import tpu as pltpu
from jax.sharding import PartitionSpec as P

MODEL_WIDTH = 2048
HEAD_SIZE = 64
BAND_LENGTH = 128


rope_base = 10000.0
norm_eps = 1e-06


def from_behind(value, axis, by):
    devices = lax.axis_size(axis)
    pairs = [(i, i + by) for i in range(devices) if 0 <= i + by < devices]
    return lax.ppermute(value, axis, pairs)


def rms_scale(inputs, gain):
    wide = inputs.astype(jnp.float32)
    scaled = wide * lax.rsqrt(jnp.mean(wide * wide, axis=-1, keepdims=True) + norm_eps)
    return (scaled * gain).astype(jnp.bfloat16)


def apply_rotary(heads, token_positions):
    freqs = rope_base ** (-jnp.arange(0, HEAD_SIZE, 2, dtype=jnp.float32) / HEAD_SIZE)
    angles = token_positions[:, None] * freqs[None, :]
    cosine = jnp.cos(angles)[:, None, :]
    sine = jnp.sin(angles)[:, None, :]
    first_half, second_half = jnp.split(heads, 2, axis=-1)
    return jnp.concatenate(
        [first_half * cosine - second_half * sine, second_half * cosine + first_half * sine],
        axis=-1,
    )


MESH = pl.DeviceIdType.MESH
F32 = jnp.float32
BF16 = jnp.bfloat16


def dot(a, b):
    return jnp.dot(a, b, preferred_element_type=F32)


def lanes_of(shape):
    return lax.broadcasted_iota(jnp.int32, shape, len(shape) - 1)


def fused_kernel(
    cap,
    sinks, ag_h, fg_h, rt_h, rw_h, fine_h, coarse_h, tf_h, wq_h, wk_h, wv_h, wo_h, ts_h,
    wg_h, wu_h, wd_h, sg_h, su_h, sd_h,
    mix_out, moe_out,
    ag, fg, rt, rw, fine, coarse, tf, wq, wk, wv, wo, ts, wg, wu, wd, sg, su, sd,
    qs, kd, vd, halo_s, halo_r, xg, mg, oh, oht, wsl, xs, hid, tokh, shh,
    mp, mrc, ms, mry, mo_own, mo_peer, rc, s1x, rx1, s1y, ry1, s2y, ry2, s2x, rx2, s3, rz, keep,
    lsem, ss, rs,
):
    me, t = lax.axis_index("ep"), lax.axis_index("tp")
    z, x, y, c = me // 2, me % 2, t // 2, t % 2
    zs = (z, z + 1 - 2 * (z % 2), (z + 2) % 4, 3 - z)
    z_peer = [{"ep": zd * 2 + x, "tp": t} for zd in zs]
    x_peer = {"ep": z * 2 + 1 - x, "tp": t}
    y_peer = {"ep": me, "tp": (1 - y) * 2 + c}
    c_peer = {"ep": me, "tp": y * 2 + 1 - c}
    n_ep = 8
    exp_dev = wg.shape[0]
    topk = rt.shape[0]
    rows = ts.shape[0]
    blocks = tf.shape[0] // rows

    loads = {}

    def load(name, src, dst):
        k = pltpu.make_async_copy(src, dst, lsem.at[len(loads)])
        k.start()
        loads[name] = k

    def need(*names):
        for name in names:
            k = loads.pop(name, None)
            if k is not None:
                done.append(name)
                k.wait()

    done = []
    pairs = [
        ("ts", ts_h, ts), ("fg", fg_h, fg), ("rt", rt_h, rt), ("rw", rw_h, rw), ("ag", ag_h, ag),
        ("tf", tf_h, tf), ("fine", fine_h, fine), ("coarse", coarse_h, coarse), ("wq", wq_h, wq),
        ("wk", wk_h, wk), ("wv", wv_h, wv), ("wo", wo_h, wo), ("sg", sg_h, sg), ("su", su_h, su),
        ("wg", wg_h, wg), ("wu", wu_h, wu), ("wd", wd_h, wd), ("sd", sd_h, sd),
    ]
    for name, a, b in pairs:
        load(name, a, b)

    barrier = pltpu.get_barrier_semaphore()
    for e in range(1, n_ep):
        pl.semaphore_signal(
            barrier, inc=1, device_id={"ep": (me + e) % n_ep, "tp": t}, device_id_type=MESH
        )
    for peer in (y_peer, c_peer):
        pl.semaphore_signal(barrier, inc=1, device_id=peer, device_id_type=MESH)

    ids = {}
    started = []

    def copy(name, src, dst, peer):
        i = ids.setdefault(name, len(ids))
        return pltpu.make_async_remote_copy(
            src_ref=src, dst_ref=dst, send_sem=ss.at[i], recv_sem=rs.at[i],
            device_id=peer, device_id_type=MESH,
        )

    def send(name, src, dst, peer):
        k = copy(name, src, dst, peer)
        k.start()
        started.append(k)

    def got(name, dst):
        copy(name, dst, dst, c_peer).wait_recv()

    def normed(wide, gain):
        return (
            wide * lax.rsqrt(jnp.mean(wide * wide, axis=-1, keepdims=True) + norm_eps) * gain
        ).astype(BF16)

    def R(d, s):
        return s * 4 + d

    own = R(0, 1)
    quarter = xg.shape[3]

    def q_of(k, cc):
        return (y if k else 1 - y) * 2 + cc

    need("ts", "fg", "rt", "rw")
    xn = normed(ts[...].astype(F32), fg[...])
    for q in range(4):
        xg[own, q] = xn[:, q * quarter : (q + 1) * quarter]
    mg[own] = jnp.concatenate([rt[...].astype(F32), rw[...]], axis=0)
    pl.semaphore_wait(barrier, n_ep + 1)

    def block_send(link, d, s, k, peer, at):
        send((link, at, k), xg.at[R(d, s), q_of(k, c)], xg.at[at, q_of(k, c)], peer)

    block_send("z", 0, 1, 1, z_peer[1], R(1, 1))
    block_send("x", 0, 1, 1, x_peer, R(0, 0))
    block_send("z", 0, 1, 1, z_peer[2], R(2, 1))
    block_send("z", 0, 1, 1, z_peer[3], R(3, 1))
    block_send("z", 0, 1, 0, z_peer[1], R(1, 1))
    block_send("x", 0, 1, 0, x_peer, R(0, 0))
    for s in (0, 1):
        for d in range(4):
            if R(d, s) != own:
                peer = {"ep": zs[d] * 2 + (x if s else 1 - x), "tp": t}
                send(("m", R(d, s)), mg.at[own], mg.at[R(d, s)], peer)

    c_list = {}

    def to_core(at, k):
        c_list[(at, k)] = True
        send(("c", at, k), xg.at[at, q_of(k, c)], xg.at[at, q_of(k, c)], c_peer)

    def to_x(d):
        send(("x", R(d, 0), 1), xg.at[R(d, 1), q_of(1, c)], xg.at[R(d, 0), q_of(1, c)], x_peer)

    def to_y(at):
        send(("y", at), xg.at[at, q_of(1, c)], xg.at[at, q_of(1, c)], y_peer)

    def arrived(link, at, k):
        got((link, at, k), xg.at[at, q_of(k, c)])

    def from_y(at):
        got(("y", at), xg.at[at, q_of(0, c)])
        to_core(at, 0)

    def from_core(at):
        for k in (1, 0):
            got(("c", at, k), xg.at[at, q_of(k, 1 - c)])

    lane = lanes_of((rows, 128))
    low = lane % 64 < 32
    left = lane < 64

    def qkv(b):
        part = slice(b * rows, (b + 1) * rows)
        nb = normed(tf[part].astype(F32), ag[...])
        base = pl.ds(me * blocks + b, 1)
        cb, sb = coarse[0, base, :], coarse[1, base, :]
        cosine = fine[0] * cb - fine[1] * sb
        sine = fine[1] * cb + fine[0] * sb
        sine = jnp.where(low, -sine, sine)

        def rot(v):
            swap = jnp.where(low, pltpu.roll(v, 96, 1), pltpu.roll(v, 32, 1))
            return v * cosine + swap * sine

        need("wk")
        kk = rot(dot(nb, wk[...]))
        need("wv")
        vv = dot(nb, wv[...])
        store_kv(kk.astype(BF16).astype(F32), vv.astype(BF16).astype(F32), (b + 1) * rows)
        if b == blocks - 1:
            halo_s[:, 0:128] = kk.astype(BF16)
            halo_s[:, 128:256] = vv.astype(BF16)
        need("wq")
        for g in range(2):
            qq = rot(dot(nb, wq[:, g * 128 : (g + 1) * 128])) * HEAD_SIZE ** (-0.5)
            qs[part, g * 128 : (g + 1) * 128] = qq.astype(BF16)

    def store_kv(kk, vv, at):
        for ref, val in ((kd, kk), (vd, vv)):
            other = pltpu.roll(val, 64, 1)
            ref[0, at : at + rows, :] = jnp.where(left, val, other).astype(BF16)
            ref[1, at : at + rows, :] = jnp.where(left, other, val).astype(BF16)

    i2 = lax.broadcasted_iota(jnp.int32, (2 * rows, 2 * rows), 0)
    band = lanes_of((2 * rows, 2 * rows)) - i2 % rows
    top = lax.broadcasted_iota(jnp.int32, (2 * rows, 1), 0) < rows

    def attend(b):
        part = slice(b * rows, (b + 1) * rows)
        outs = []
        visible = (band > 0) & (band <= rows)
        if b == 0:
            visible = visible & ((lanes_of((2 * rows, 2 * rows)) >= rows) | (me > 0))
        for g in range(2):
            q2 = qs[part, g * 128 : (g + 1) * 128]
            zero = jnp.zeros_like(q2)
            qq = jnp.concatenate([jnp.where(left, q2, zero), jnp.where(left, zero, q2)], axis=0)
            score = lax.dot_general(
                qq, kd[g, b * rows : (b + 2) * rows, :], (((1,), (1,)), ((), ())),
                preferred_element_type=F32,
            )
            score = jnp.where(visible, score, -jnp.inf)
            sink = jnp.where(top, sinks[2 * g], sinks[2 * g + 1])
            peak = jnp.maximum(jnp.max(score, axis=-1, keepdims=True), sink)
            expo = jnp.exp(score - peak)
            total = jnp.sum(expo, axis=-1, keepdims=True) + jnp.exp(sink - peak)
            weights = (expo * (1.0 / total)).astype(BF16)
            o = dot(weights, vd[g, b * rows : (b + 2) * rows, :])
            outs.append(jnp.where(left, o[:rows], o[rows:]).astype(BF16))
        att = jnp.concatenate(outs, axis=1)
        need("wo")
        for n in range(4):
            mp[b, :, n * 512 : (n + 1) * 512] = dot(att, wo[:, n * 512 : (n + 1) * 512]).astype(BF16)

    def onehots():
        for s in (0, 1):
            for d in range(4):
                if R(d, s) != own:
                    got(("m", R(d, s)), mg.at[R(d, s)])
        before = (
            lax.broadcasted_iota(jnp.int32, (rows, rows), 0)
            < lax.broadcasted_iota(jnp.int32, (rows, rows), 1)
        ).astype(F32).astype(BF16)
        hits, vals = [], []
        for r in range(n_ep):
            for e in range(exp_dev):
                named = mg[r, 0:topk, :] == (me * exp_dev + e).astype(F32)
                hits.append(jnp.sum(named.astype(F32), axis=0, keepdims=True))
                vals.append(
                    jnp.sum(jnp.where(named, mg[r, topk : 2 * topk, :], 0.0), axis=0, keepdims=True)
                )
        ranks = dot(jnp.concatenate(hits, axis=0).astype(BF16), before)
        slot = lax.broadcasted_iota(jnp.int32, (cap, rows), 0).astype(F32)
        for r in range(n_ep):
            both = []
            for e in range(exp_dev):
                i = r * exp_dev + e
                at = (slot == ranks[i : i + 1, :]) & (hits[i] > 0.0)
                both.append(at.astype(F32))
                wsl[r, e] = jnp.sum(jnp.where(at, vals[i], 0.0), axis=1, keepdims=True)
            full = jnp.concatenate(both, axis=0)
            oh[r] = full.astype(BF16)
            turned = full.T
            for e in range(exp_dev):
                oht[r, e] = jnp.where(lanes_of(turned.shape) // cap == e, turned, 0.0).astype(BF16)

    def shared_hidden():
        need("sg", "su")
        g = jnp.zeros((rows, sg.shape[1]), F32)
        u = jnp.zeros((rows, sg.shape[1]), F32)
        for q in range(4):
            part = slice(q * quarter, (q + 1) * quarter)
            g = g + dot(xg[own, q], sg[part, :])
            u = u + dot(xg[own, q], su[part, :])
        shh[...] = (g / (1.0 + jnp.exp(-g)) * u).astype(BF16)

    half = 4 * cap

    def dispatch(h, group):
        for i, r in enumerate(group):
            for q in range(4):
                v = dot(oh[r], xg[r, q]).astype(BF16)
                for e in range(exp_dev):
                    xs[e, h * half + i * cap : h * half + (i + 1) * cap,
                       q * quarter : (q + 1) * quarter] = v[e * cap : (e + 1) * cap]

    def gate_up(h, group, e):
        need("wg", "wu")
        rin = slice(h * half, (h + 1) * half)
        wcol = jnp.concatenate([wsl[r, e] for r in group], axis=0)
        for n in range(2):
            cs = slice(n * 256, (n + 1) * 256)
            g = dot(xs[e, rin, :], wg[e, :, cs])
            u = dot(xs[e, rin, :], wu[e, :, cs])
            hh = (g / (1.0 + jnp.exp(-g)) * u * wcol).astype(BF16)
            for i, r in enumerate(group):
                hid[r * rows + e * cap : r * rows + (e + 1) * cap, cs] = hh[i * cap : (i + 1) * cap]

    def to_tokens(group):
        width = hid.shape[1]
        for r in group:
            for e in range(exp_dev):
                tokh[r * rows : (r + 1) * rows, e * width : (e + 1) * width] = dot(
                    oht[r, e], hid[r * rows : (r + 1) * rows, :]
                ).astype(BF16)

    ysel = (1 - y, y)

    def down(jj, yr, dst, cc):
        need("wd", "sd")
        width = hid.shape[1]
        base = pl.multiple_of((ysel[yr] * 2 + cc) * 512 + jj * 256, 256)
        cs = pl.ds(base, 256)
        for rb in range(4):
            part = slice(rb * 256, (rb + 1) * 256)
            o = dot(tokh[part, 0:width], wd[0, :, cs]) + dot(tokh[part, width : 2 * width], wd[1, :, cs])
            if rb == own * rows // 256:
                extra = dot(shh[...], sd[:, cs])
                o = jnp.concatenate([o[:rows] + extra, o[rows:]], axis=0)
            dst[jj, yr, 0, part, :] = o[:, 0:128].astype(BF16)
            dst[jj, yr, 1, part, :] = o[:, 128:256].astype(BF16)

    def core_send(jj):
        for yr in range(2):
            for o in range(2):
                send(("rc", jj, yr, o), mo_peer.at[jj, yr, o], rc.at[jj, yr, o], c_peer)

    def both(jj, yr, o, part):
        return mo_own[jj, yr, o, part, :].astype(F32) + rc[jj, yr, o, part, :].astype(F32)

    far, near = slice(0, 512), slice(512, 1024)

    def stage1(jj):
        for yr in range(2):
            for o in range(2):
                got(("rc", jj, yr, o), rc.at[jj, yr, o])
        for yr in range(2):
            s1x[jj, yr] = both(jj, yr, 0, far).astype(BF16)
        send(("rx1", jj), s1x.at[jj], rx1.at[jj], x_peer)
        s1y[jj] = both(jj, 0, 1, slice(0, 1024)).astype(BF16)
        send(("ry1", jj), s1y.at[jj], ry1.at[jj], y_peer)

    def stage2(jj):
        got(("rx1", jj), rx1.at[jj])
        s2y[jj] = (both(jj, 0, 0, near) + rx1[jj, 0].astype(F32)).astype(BF16)
        send(("ry2", jj), s2y.at[jj], ry2.at[jj], y_peer)
        got(("ry1", jj), ry1.at[jj])
        s2x[jj] = (both(jj, 1, 1, far) + ry1[jj, far, :].astype(F32)).astype(BF16)
        send(("rx2", jj), s2x.at[jj], rx2.at[jj], x_peer)

    def stage3(jj, o):
        if o == 0:
            got(("ry2", jj), ry2.at[jj])
        else:
            got(("rx2", jj), rx2.at[jj])
        for d in (2, 3, 1, 0):
            part = slice(512 + d * 128, 512 + (d + 1) * 128)
            here = slice(d * 128, (d + 1) * 128)
            v = both(jj, 1, o, part)
            if o == 0:
                v = v + rx1[jj, 1, here, :].astype(F32) + ry2[jj, here, :].astype(F32)
            else:
                v = v + ry1[jj, part, :].astype(F32) + rx2[jj, here, :].astype(F32)
            if d:
                s3[jj, o, d - 1] = v.astype(BF16)
                send(("rz", jj, o, d), s3.at[jj, o, d - 1], rz.at[jj, o, d - 1], z_peer[d])
            else:
                keep[jj, o] = v

    def final(jj, o):
        v = keep[jj, o]
        for d in (1, 2, 3):
            got(("rz", jj, o, d), rz.at[jj, o, d - 1])
            v = v + rz[jj, o, d - 1].astype(F32)
        at = jj * 256 + o * 128
        moe_out[:, at : at + 128] = v.astype(BF16)

    need("ag", "tf", "fine", "coarse")
    qkv(3)

    @pl.when(me < n_ep - 1)
    def _():
        copy("halo", halo_s, halo_r, {"ep": (me + 1) % n_ep, "tp": t}).start()

    arrived("z", R(1, 1), 1)
    to_x(1)
    to_core(R(1, 1), 1)
    arrived("x", R(0, 0), 1)
    to_core(R(0, 0), 1)
    qkv(0)
    qkv(1)
    arrived("z", R(2, 1), 1)
    to_x(2)
    to_y(R(2, 1))
    to_core(R(2, 1), 1)
    arrived("x", R(0, 0), 0)
    to_core(R(0, 0), 0)
    qkv(2)
    onehots()
    arrived("z", R(3, 1), 1)
    to_x(3)
    to_y(R(3, 1))
    to_core(R(3, 1), 1)
    arrived("z", R(1, 1), 0)
    to_core(R(1, 1), 0)
    attend(1)
    arrived("x", R(1, 0), 1)
    to_y(R(1, 0))
    to_core(R(1, 0), 1)
    attend(2)
    arrived("x", R(2, 0), 1)
    to_y(R(2, 0))
    to_core(R(2, 0), 1)
    attend(3)

    @pl.when(me == 0)
    def _():
        halo_r[...] = jnp.zeros_like(halo_r)

    @pl.when(me > 0)
    def _():
        got("halo", halo_r)

    store_kv(halo_r[:, 0:128].astype(F32), halo_r[:, 128:256].astype(F32), 0)
    attend(0)
    arrived("x", R(3, 0), 1)
    to_y(R(3, 0))
    to_core(R(3, 0), 1)
    for k in (0, 1):
        send(("mrc", k), mp.at[ysel[k] * 2 + 1 - c], mrc.at[k], c_peer)
    shared_hidden()
    from_y(R(2, 1))
    from_y(R(3, 1))
    got(("mrc", 0), mrc.at[0])
    ms[...] = (mp[ysel[0] * 2 + c].astype(F32) + mrc[0].astype(F32)).astype(BF16)
    send("mry", ms, mry, y_peer)
    from_y(R(1, 0))
    first = (R(0, 1), R(0, 0), R(1, 1), R(1, 0))
    second = (R(2, 1), R(3, 1), R(2, 0), R(3, 0))
    for r in first[1:]:
        from_core(r)
    dispatch(0, first)
    gate_up(0, first, 0)
    from_y(R(2, 0))
    gate_up(0, first, 1)
    from_y(R(3, 0))
    to_tokens(first)
    for r in second:
        from_core(r)
    dispatch(1, second)
    gate_up(1, second, 0)
    gate_up(1, second, 1)
    to_tokens(second)
    for jj in range(2):
        for yr in range(2):
            down(jj, yr, mo_peer, 1 - c)
        core_send(jj)
        for yr in range(2):
            down(jj, yr, mo_own, c)
        stage1(jj)
    stage2(0)
    got(("mrc", 1), mrc.at[1])
    got("mry", mry)
    mix_out[...] = (
        mp[ysel[1] * 2 + c].astype(F32) + mrc[1].astype(F32) + mry[...].astype(F32)
    ).astype(BF16)
    stage3(0, 0)
    stage3(0, 1)
    stage2(1)
    final(0, 0)
    final(0, 1)
    stage3(1, 0)
    stage3(1, 1)
    final(1, 0)
    final(1, 1)

    @pl.when(me < n_ep - 1)
    def _():
        copy("halo", halo_s, halo_r, {"ep": (me + 1) % n_ep, "tp": t}).wait_send()

    for k in started:
        k.wait_send()
    assert not loads and len(ids) <= ss.shape[0]


def rope_tables(tokens, rows):
    freqs = rope_base ** (-np.arange(0, HEAD_SIZE, 2) / HEAD_SIZE)
    freqs = np.tile(freqs, 128 // len(freqs))
    fine = np.arange(rows)[:, None] * freqs[None, :]
    coarse = np.arange(0, tokens, rows)[:, None] * freqs[None, :]
    return [
        jnp.asarray(np.stack([np.cos(a), np.sin(a)]), dtype=jnp.float32) for a in (fine, coarse)
    ]


def fused(tf, ag, wq, wk, wv, sink, wo, ts, fg, routes, rweight, wg, wu, wd, sg, su, sd):
    n_ep = lax.axis_size("ep")
    rows, wide = ts.shape
    exp_dev, _, hidden = wg.shape
    cap = max(2, 2 * rows * routes.shape[1] // (exp_dev * n_ep))
    mrows = tf.shape[0] // 4
    fine, coarse = rope_tables(tf.shape[0] * n_ep, rows)
    args = (
        sink, ag.reshape(1, -1), fg.reshape(1, -1), routes.T, rweight.T, fine, coarse,
        tf, wq, wk, wv, wo, ts, wg, wu, wd, sg, su, sd,
    )
    vm = pl.BlockSpec(memory_space=pltpu.VMEM)
    hbm = pl.BlockSpec(memory_space=pl.ANY)
    v = pltpu.VMEM
    dma = pltpu.SemaphoreType.DMA
    qw = wide // 4
    scratch = [v(a.shape, a.dtype) for a in args[1:]] + [
        v((tf.shape[0], 256), BF16),
        v((2, tf.shape[0] + rows, 128), BF16),
        v((2, tf.shape[0] + rows, 128), BF16),
        v((rows, 256), BF16),
        v((rows, 256), BF16),
        v((n_ep, 4, rows, qw), BF16),
        v((n_ep, 2 * routes.shape[1], rows), F32),
        v((n_ep, exp_dev * cap, rows), BF16),
        v((n_ep, exp_dev, rows, exp_dev * cap), BF16),
        v((n_ep, exp_dev, cap, 1), F32),
        v((exp_dev, n_ep * cap, wide), BF16),
        v((n_ep * exp_dev * cap, hidden), BF16),
        v((n_ep * rows, exp_dev * hidden), BF16),
        v((rows, sg.shape[1]), BF16),
        v((4, mrows, wide), BF16),
        v((2, mrows, wide), BF16),
        v((mrows, wide), BF16),
        v((mrows, wide), BF16),
        v((2, 2, 2, n_ep * rows, 128), BF16),
        v((2, 2, 2, n_ep * rows, 128), BF16),
        v((2, 2, 2, n_ep * rows, 128), BF16),
        v((2, 2, 4 * rows, 128), BF16),
        v((2, 2, 4 * rows, 128), BF16),
        v((2, 8 * rows, 128), BF16),
        v((2, 8 * rows, 128), BF16),
        v((2, 4 * rows, 128), BF16),
        v((2, 4 * rows, 128), BF16),
        v((2, 4 * rows, 128), BF16),
        v((2, 4 * rows, 128), BF16),
        v((2, 2, 3, rows, 128), BF16),
        v((2, 2, 3, rows, 128), BF16),
        v((2, 2, rows, 128), F32),
        dma((18,)), dma((72,)), dma((72,)),
    ]
    moe_out_shape = jax.ShapeDtypeStruct((rows, qw), BF16)
    mix_out_shape = jax.ShapeDtypeStruct((mrows, wide), BF16)
    return pl.pallas_call(
        functools.partial(fused_kernel, cap),
        out_shape=(mix_out_shape, moe_out_shape),
        in_specs=[pl.BlockSpec(memory_space=pltpu.SMEM)] + [hbm] * (len(args) - 1),
        out_specs=(vm, vm),
        scratch_shapes=scratch,
        compiler_params=pltpu.CompilerParams(
            collective_id=0, has_side_effects=True, vmem_limit_bytes=60 * 1024 * 1024
        ),
        name="fused",
    )(*args)


def local(
    tokens_first,
    attn_gain,
    w_query,
    key_matrix,
    value_matrix,
    head_sink_logit,
    w_output,
    tokens_second,
    ffn_gain,
    routes,
    route_weight,
    w_gate_exp,
    w_up_exp,
    w_down_exp,
    w_gate_shared,
    w_up_shared,
    w_down_shared,
):
    if lax.axis_size("ep") == 8 and lax.axis_size("tp") == 4:
        return fused(
            tokens_first, attn_gain, w_query, key_matrix, value_matrix, head_sink_logit, w_output,
            tokens_second, ffn_gain, routes, route_weight, w_gate_exp, w_up_exp, w_down_exp,
            w_gate_shared, w_up_shared, w_down_shared,
        )
    rows_first = tokens_first.shape[0]
    norm_input = rms_scale(tokens_first, attn_gain)
    offset = lax.axis_index("ep") * rows_first
    token_positions = (offset + jnp.arange(rows_first, dtype=jnp.int32)).astype(jnp.float32)
    head_count = w_query.shape[1] // HEAD_SIZE
    key_heads = key_matrix.shape[1] // HEAD_SIZE
    head_group = head_count // key_heads
    query_rows = apply_rotary(
        jnp.dot(norm_input, w_query, preferred_element_type=jnp.float32).reshape(
            rows_first, head_count, HEAD_SIZE
        ),
        token_positions,
    ).astype(jnp.bfloat16)
    keys_local = apply_rotary(
        jnp.dot(norm_input, key_matrix, preferred_element_type=jnp.float32).reshape(
            rows_first, key_heads, HEAD_SIZE
        ),
        token_positions,
    ).astype(jnp.bfloat16)
    values_local = (
        jnp.dot(norm_input, value_matrix, preferred_element_type=jnp.float32)
        .astype(jnp.bfloat16)
        .reshape(rows_first, key_heads, HEAD_SIZE)
    )
    keys_before, values_before = from_behind(
        (keys_local[rows_first - BAND_LENGTH :], values_local[rows_first - BAND_LENGTH :]),
        "ep",
        1,
    )
    keys_all = jnp.concatenate([keys_before, keys_local], axis=0)
    values_all = jnp.concatenate([values_before, values_local], axis=0)
    band = BAND_LENGTH
    bands = rows_first // band

    def windows(padded):
        return jnp.concatenate(
            [
                padded[:rows_first].reshape(bands, band, key_heads, HEAD_SIZE),
                padded[band:].reshape(bands, band, key_heads, HEAD_SIZE),
            ],
            axis=1,
        )

    sink_scores = head_sink_logit.reshape(key_heads, head_group)[None, :, :, None, None]
    scores = jnp.einsum(
        "bqhgd,bkhd->bhgqk",
        query_rows.reshape(bands, band, key_heads, head_group, HEAD_SIZE),
        windows(keys_all),
        preferred_element_type=jnp.float32,
    ) * HEAD_SIZE ** (-0.5)
    offsets = (
        band
        + jnp.arange(band, dtype=jnp.int32)[:, None]
        - jnp.arange(2 * band, dtype=jnp.int32)[None, :]
    )
    key_pos = (
        offset
        + (jnp.arange(bands, dtype=jnp.int32)[:, None] - 1) * band
        + jnp.arange(2 * band, dtype=jnp.int32)[None, :]
    )
    visible = ((offsets >= 0) & (offsets < band))[None] & (key_pos >= 0)[:, None, :]
    scores = jnp.where(visible[:, None, None], scores, -jnp.inf)
    peak = jnp.maximum(jnp.max(scores, axis=-1, keepdims=True), sink_scores)
    expo = jnp.exp(scores - peak)
    total = jnp.sum(expo, axis=-1, keepdims=True) + jnp.exp(sink_scores - peak)
    weights = (expo / total).astype(jnp.bfloat16)
    attended = (
        jnp.einsum(
            "bhgqk,bkhd->bqhgd", weights, windows(values_all), preferred_element_type=jnp.float32
        )
        .astype(jnp.bfloat16)
        .reshape(rows_first, head_count * HEAD_SIZE)
    )
    mixer_out = lax.psum_scatter(
        jnp.dot(attended, w_output, preferred_element_type=jnp.float32).astype(jnp.bfloat16),
        "tp",
        scatter_dimension=0,
        tiled=True,
    )
    rows_second = tokens_second.shape[0]
    topk = routes.shape[1]
    exp_dev = w_gate_exp.shape[0]
    n_expdev = lax.axis_size("ep")
    experts = exp_dev * n_expdev
    capacity = max(2, 2 * rows_second * topk // experts)
    slot_count = experts * capacity
    normed_second = rms_scale(tokens_second, ffn_gain)
    flat = routes.reshape(-1)
    onehot = (flat[:, None] == jnp.arange(experts, dtype=jnp.int32)[None, :]).astype(jnp.int32)
    ranks = jnp.sum((jnp.cumsum(onehot, axis=0) - onehot) * onehot, axis=1)
    slots = flat * capacity + ranks
    match = (jnp.arange(slot_count, dtype=jnp.int32)[:, None] == slots[None, :]).reshape(
        slot_count, rows_second, topk
    )
    dispatch = jnp.sum(match.astype(jnp.float32), axis=2).astype(jnp.bfloat16)
    combine = jnp.sum(match.astype(jnp.float32) * route_weight[None, :, :], axis=2)
    width = normed_second.shape[1] // lax.axis_size("tp")
    feature_slice = lax.dynamic_slice_in_dim(normed_second, lax.axis_index("tp") * width, width, 1)
    outgoing = jnp.dot(dispatch, feature_slice, preferred_element_type=jnp.float32).astype(
        jnp.bfloat16
    )
    arrived = lax.all_to_all(outgoing, "ep", split_axis=0, concat_axis=0, tiled=True)
    piece = lax.all_gather(arrived, "tp", axis=1, tiled=True)
    cols = piece.shape[1]
    part = piece.reshape(n_expdev, exp_dev, capacity, cols)
    gate_pre = jnp.einsum("sjcd,jdf->sjcf", part, w_gate_exp, preferred_element_type=jnp.float32)
    up_pre = jnp.einsum("sjcd,jdf->sjcf", part, w_up_exp, preferred_element_type=jnp.float32)
    hidden = (jax.nn.silu(gate_pre) * up_pre).astype(jnp.bfloat16)
    shared_hidden = (
        jax.nn.silu(jnp.dot(normed_second, w_gate_shared, preferred_element_type=jnp.float32))
        * jnp.dot(normed_second, w_up_shared, preferred_element_type=jnp.float32)
    ).astype(jnp.bfloat16)
    routed_term = jnp.einsum(
        "sjcf,jfd->dsjc", hidden, w_down_exp, preferred_element_type=jnp.float32
    ).reshape(lax.axis_size("tp") * (MODEL_WIDTH // lax.axis_size("tp")), slot_count)
    shared_term = lax.dot_general(
        w_down_shared, shared_hidden, (((0,), (1,)), ((), ())), preferred_element_type=jnp.float32
    )
    summed = lax.psum_scatter(
        jnp.concatenate([routed_term, shared_term], axis=1).astype(jnp.bfloat16),
        "tp",
        scatter_dimension=0,
        tiled=True,
    ).astype(jnp.float32)
    routed_part = summed[:, :slot_count].astype(jnp.bfloat16)
    returned = lax.all_to_all(routed_part, "ep", split_axis=1, concat_axis=1, tiled=True)
    weighted = lax.dot_general(
        combine,
        returned.astype(jnp.float32),
        (((0,), (1,)), ((), ())),
        precision=lax.Precision.HIGHEST,
    )
    moe_out = (weighted + summed[:, slot_count:].T).astype(jnp.bfloat16)
    return (mixer_out, moe_out)


def solution(mesh):
    in_specs = (
        P("ep", None),
        P(),
        P(None, "tp"),
        P(None, "tp"),
        P(None, "tp"),
        P("tp"),
        P("tp", None),
        P("ep", None),
        P(),
        P("ep", None),
        P("ep", None),
        P("ep", None, "tp"),
        P("ep", None, "tp"),
        P("ep", "tp", None),
        P(None, "tp"),
        P(None, "tp"),
        P("tp", None),
    )
    out_specs = (P(("ep", "tp"), None), P("ep", "tp"))
    return jax.shard_map(local, mesh=mesh, in_specs=in_specs, out_specs=out_specs, check_vma=False)
```

time: 117 us -> 78.1 us (0.67)
  Pallas kernels: 93.1 us -> 73.8 us
  other arithmetic: 8 us -> 0 us
  matrix products: 6.33 us -> 0 us
  local copies, waits for them, and re-layouts: 8.14 us -> 3.45 us
    pallas_call x3 -> x1, Pallas kernels: 93.1 us -> 73.8 us  [fused(): pl.pallas_call(functools.partial(fused_kernel, cap), out_shape=(mix_out_s...]
    dot_general x6 -> x0, matrix products: 6.33 us -> none  [the longest x1 1.55 us: local(): jnp.einsum('bhgqk,bkhd->bqhgd', weights, windows(values_all), preferred_e...]
    reduce_sum x3 -> x0, other arithmetic: 3.76 us -> none  [the longest x2 3.45 us: rms_scale(): jnp.mean(wide * wide, axis=-1, keepdims=True) + norm_eps]
    convert_element_type x3 -> x0, other arithmetic: 1.93 us -> none  [the longest x1 1.24 us: rms_scale(): return (scaled * gain).astype(jnp.bfloat16)]
    slice x4 -> x0, local copies, waits for them, and re-layouts: 1.58 us -> none  [the longest x2 1.47 us: local(): values_before = before[:, split:].reshape(BAND_LENGTH, key_heads, HEAD_SIZE)]
    unnamed x24 -> x2, local copies, waits for them, and re-layouts: 4.33 us -> 3.45 us
where the time goes in v1:
time: 78.1 us; the launch traced here: 77.9 us
  Pallas kernels  73.8 us (94%)
  local copies, waits for them, and re-layouts  3.45 us (4%)
    pallas_call x1, Pallas kernels, fused(): pl.pallas_call(functools.partial(fused_kernel, cap), out_shape=(mix_out_s...  73.8 us
    unnamed x2, local copies, waits for them, and re-layouts  3.45 us

profile of v1, /device:TPU:0, one launch (start us, length us, event | category | flops | bytes accessed | tf_op | source)
XLA Modules:
  0.0 77.9 jit_solution(7585856451653529015)
XLA Ops:
  0.6 73.8 %fused.1 = (bf16[128,2048]{1,0:T(8,128)(2,1)}, bf16[128,512]{1,0:T(8,128)(2,1)}) custom-call(f32[4]{0:T(128)} %sinks.1, f32[1,2048]{1,0:T(1,128)} %bitcast.4, f32[1,2048]{1,0:T(1,128)} %bitcast.5, s32[4,128]{1,0:T(4,128)} %bitcast.6, f32[4,128]{1,0:T(4,128)} %bitcast.7, f32[2,128,128]{2,1,0:T(8,128)} %constant.4.clone.fine_h, ...), custom_call_target="tpu_custom_call" | custom-call | tf_op jit(solution)/shard_map/fused/pallas_call | solution.py:569
  74.5 1.9 %copy.23 = bf16[128,2048]{1,0:T(8,128)(2,1)} copy(bf16[128,2048]{1,0:T(8,128)(2,1)} %get-tuple-element.4) | data formatting | bytes 1048576
  76.3 1.6 %copy.24 = bf16[128,512]{1,0:T(8,128)(2,1)} copy(bf16[128,512]{1,0:T(8,128)(2,1)} %get-tuple-element.5) | data formatting | bytes 262144

commit v2 on v1

--- a/solution.py
+++ b/solution.py
@@ -49,6 +49,14 @@
     return jnp.dot(a, b, preferred_element_type=F32)
 
 
+def scoped(f):
+    def call(*a):
+        with jax.named_scope("_".join([f.__name__] + [str(v) for v in a if isinstance(v, int)])):
+            return f(*a)
+
+    return call
+
+
 def lanes_of(shape):
     return lax.broadcasted_iota(jnp.int32, shape, len(shape) - 1)
 
@@ -60,7 +68,7 @@
     mix_out, moe_out,
     ag, fg, rt, rw, fine, coarse, tf, wq, wk, wv, wo, ts, wg, wu, wd, sg, su, sd,
     qs, kd, vd, halo_s, halo_r, xg, mg, oh, oht, wsl, xs, hid, tokh, shh,
-    mp, mrc, ms, mry, mo_own, mo_peer, rc, s1x, rx1, s1y, ry1, s2y, ry2, s2x, rx2, s3, rz, keep,
+    mp, mrc, ms, mry, mo_own, mo_peer, rc, s1x, rx1, s2y, ry2, s3, rz, keep,
     lsem, ss, rs,
 ):
     me, t = lax.axis_index("ep"), lax.axis_index("tp")
@@ -131,8 +139,10 @@
             wide * lax.rsqrt(jnp.mean(wide * wide, axis=-1, keepdims=True) + norm_eps) * gain
         ).astype(BF16)
 
+    turn = (0, 3, 1, 2)
+
     def R(d, s):
-        return s * 4 + d
+        return turn[d] * 2 + s
 
     own = R(0, 1)
     quarter = xg.shape[3]
@@ -140,55 +150,71 @@
     def q_of(k, cc):
         return (y if k else 1 - y) * 2 + cc
 
-    need("ts", "fg", "rt", "rw")
-    xn = normed(ts[...].astype(F32), fg[...])
-    for q in range(4):
-        xg[own, q] = xn[:, q * quarter : (q + 1) * quarter]
-    mg[own] = jnp.concatenate([rt[...].astype(F32), rw[...]], axis=0)
-    pl.semaphore_wait(barrier, n_ep + 1)
-
-    def block_send(link, d, s, k, peer, at):
-        send((link, at, k), xg.at[R(d, s), q_of(k, c)], xg.at[at, q_of(k, c)], peer)
-
-    block_send("z", 0, 1, 1, z_peer[1], R(1, 1))
-    block_send("x", 0, 1, 1, x_peer, R(0, 0))
-    block_send("z", 0, 1, 1, z_peer[2], R(2, 1))
-    block_send("z", 0, 1, 1, z_peer[3], R(3, 1))
-    block_send("z", 0, 1, 0, z_peer[1], R(1, 1))
-    block_send("x", 0, 1, 0, x_peer, R(0, 0))
+    @scoped
+    def norm_second():
+        need("ts", "fg", "rt", "rw")
+        xn = normed(ts[...].astype(F32), fg[...])
+        for q in range(4):
+            xg[own, q] = xn[:, q * quarter : (q + 1) * quarter]
+        mg[own] = jnp.concatenate([rt[...].astype(F32), rw[...]], axis=0)
+
+    norm_second()
+
+    @scoped
+    def barrier_wait():
+        pl.semaphore_wait(barrier, n_ep + 1)
+
+    barrier_wait()
+
     for s in (0, 1):
         for d in range(4):
             if R(d, s) != own:
                 peer = {"ep": zs[d] * 2 + (x if s else 1 - x), "tp": t}
                 send(("m", R(d, s)), mg.at[own], mg.at[R(d, s)], peer)
 
-    c_list = {}
-
-    def to_core(at, k):
-        c_list[(at, k)] = True
-        send(("c", at, k), xg.at[at, q_of(k, c)], xg.at[at, q_of(k, c)], c_peer)
-
-    def to_x(d):
-        send(("x", R(d, 0), 1), xg.at[R(d, 1), q_of(1, c)], xg.at[R(d, 0), q_of(1, c)], x_peer)
-
-    def to_y(at):
-        send(("y", at), xg.at[at, q_of(1, c)], xg.at[at, q_of(1, c)], y_peer)
-
-    def arrived(link, at, k):
-        got((link, at, k), xg.at[at, q_of(k, c)])
-
-    def from_y(at):
-        got(("y", at), xg.at[at, q_of(0, c)])
-        to_core(at, 0)
-
+    parts = 2
+    sub = rows // parts
+
+    def piece(at, q, p):
+        return xg.at[at, q, p * sub : (p + 1) * sub, :]
+
+    def block_send(link, k, peer, at, p):
+        q = q_of(k, c)
+        send((link, at, k, p), piece(own, q, p), piece(at, q, p), peer)
+
+    for p in range(parts):
+        block_send("z", 1, z_peer[2], R(2, 1), p)
+        block_send("x", 1, x_peer, R(0, 0), p)
+    for p in range(parts):
+        block_send("z", 1, z_peer[3], R(3, 1), p)
+        block_send("x", 0, x_peer, R(0, 0), p)
+    for p in range(parts):
+        block_send("z", 1, z_peer[1], R(1, 1), p)
+        block_send("z", 0, z_peer[1], R(1, 1), p)
+
+    def arrive(link, d, s, k, p, *onward):
+        at, q = R(d, s), q_of(k, c)
+        here = piece(at, q, p)
+        with jax.named_scope("%s_d%d_s%d_k%d_p%d" % (link, d, s, k, p)):
+            got((link, at, k, p), here)
+        for way in onward:
+            if way == "x":
+                send(("x", R(d, 0), k, p), here, piece(R(d, 0), q, p), x_peer)
+            else:
+                send(("y", at, 0, p), here, here, y_peer)
+        send(("c", at, k, p), here, here, c_peer)
+
+    @scoped
     def from_core(at):
-        for k in (1, 0):
-            got(("c", at, k), xg.at[at, q_of(k, 1 - c)])
+        for p in range(parts):
+            for k in (1, 0):
+                got(("c", at, k, p), piece(at, q_of(k, 1 - c), p))
 
     lane = lanes_of((rows, 128))
     low = lane % 64 < 32
     left = lane < 64
 
+    @scoped
     def qkv(b):
         part = slice(b * rows, (b + 1) * rows)
         nb = normed(tf[part].astype(F32), ag[...])
@@ -225,6 +251,7 @@
     band = lanes_of((2 * rows, 2 * rows)) - i2 % rows
     top = lax.broadcasted_iota(jnp.int32, (2 * rows, 1), 0) < rows
 
+    @scoped
     def attend(b):
         part = slice(b * rows, (b + 1) * rows)
         outs = []
@@ -252,6 +279,7 @@
         for n in range(4):
             mp[b, :, n * 512 : (n + 1) * 512] = dot(att, wo[:, n * 512 : (n + 1) * 512]).astype(BF16)
 
+    @scoped
     def onehots():
         for s in (0, 1):
             for d in range(4):
@@ -284,6 +312,7 @@
             for e in range(exp_dev):
                 oht[r, e] = jnp.where(lanes_of(turned.shape) // cap == e, turned, 0.0).astype(BF16)
 
+    @scoped
     def shared_hidden():
         need("sg", "su")
         g = jnp.zeros((rows, sg.shape[1]), F32)
@@ -294,31 +323,35 @@
             u = u + dot(xg[own, q], su[part, :])
         shh[...] = (g / (1.0 + jnp.exp(-g)) * u).astype(BF16)
 
-    half = 4 * cap
-
-    def dispatch(h, group):
-        for i, r in enumerate(group):
+    def pair(d):
+        return (R(d, 0), R(d, 1))
+
+    @scoped
+    def dispatch(d):
+        for i, r in enumerate(pair(d)):
             for q in range(4):
                 v = dot(oh[r], xg[r, q]).astype(BF16)
                 for e in range(exp_dev):
-                    xs[e, h * half + i * cap : h * half + (i + 1) * cap,
-                       q * quarter : (q + 1) * quarter] = v[e * cap : (e + 1) * cap]
-
-    def gate_up(h, group, e):
+                    xs[e, i * cap : (i + 1) * cap, q * quarter : (q + 1) * quarter] = v[
+                        e * cap : (e + 1) * cap
+                    ]
+
+    @scoped
+    def gate_up(d, e):
         need("wg", "wu")
-        rin = slice(h * half, (h + 1) * half)
-        wcol = jnp.concatenate([wsl[r, e] for r in group], axis=0)
-        for n in range(2):
+        wcol = jnp.concatenate([wsl[r, e] for r in pair(d)], axis=0)
+        for n in range(hid.shape[1] // 256):
             cs = slice(n * 256, (n + 1) * 256)
-            g = dot(xs[e, rin, :], wg[e, :, cs])
-            u = dot(xs[e, rin, :], wu[e, :, cs])
+            g = dot(xs[e], wg[e, :, cs])
+            u = dot(xs[e], wu[e, :, cs])
             hh = (g / (1.0 + jnp.exp(-g)) * u * wcol).astype(BF16)
-            for i, r in enumerate(group):
+            for i, r in enumerate(pair(d)):
                 hid[r * rows + e * cap : r * rows + (e + 1) * cap, cs] = hh[i * cap : (i + 1) * cap]
 
-    def to_tokens(group):
+    @scoped
+    def to_tokens(d):
         width = hid.shape[1]
-        for r in group:
+        for r in pair(d):
             for e in range(exp_dev):
                 tokh[r * rows : (r + 1) * rows, e * width : (e + 1) * width] = dot(
                     oht[r, e], hid[r * rows : (r + 1) * rows, :]
@@ -326,74 +359,91 @@
 
     ysel = (1 - y, y)
 
-    def down(jj, yr, dst, cc):
+    @scoped
+    def down(d, yr, peer):
         need("wd", "sd")
+        i = turn[d]
+        cc = 1 - c if peer else c
+        out = mo_peer if peer else mo_own
         width = hid.shape[1]
-        base = pl.multiple_of((ysel[yr] * 2 + cc) * 512 + jj * 256, 256)
-        cs = pl.ds(base, 256)
-        for rb in range(4):
-            part = slice(rb * 256, (rb + 1) * 256)
-            o = dot(tokh[part, 0:width], wd[0, :, cs]) + dot(tokh[part, width : 2 * width], wd[1, :, cs])
-            if rb == own * rows // 256:
-                extra = dot(shh[...], sd[:, cs])
-                o = jnp.concatenate([o[:rows] + extra, o[rows:]], axis=0)
-            dst[jj, yr, 0, part, :] = o[:, 0:128].astype(BF16)
-            dst[jj, yr, 1, part, :] = o[:, 128:256].astype(BF16)
-
-    def core_send(jj):
-        for yr in range(2):
-            for o in range(2):
-                send(("rc", jj, yr, o), mo_peer.at[jj, yr, o], rc.at[jj, yr, o], c_peer)
-
-    def both(jj, yr, o, part):
-        return mo_own[jj, yr, o, part, :].astype(F32) + rc[jj, yr, o, part, :].astype(F32)
-
-    far, near = slice(0, 512), slice(512, 1024)
-
-    def stage1(jj):
-        for yr in range(2):
-            for o in range(2):
-                got(("rc", jj, yr, o), rc.at[jj, yr, o])
-        for yr in range(2):
-            s1x[jj, yr] = both(jj, yr, 0, far).astype(BF16)
-        send(("rx1", jj), s1x.at[jj], rx1.at[jj], x_peer)
-        s1y[jj] = both(jj, 0, 1, slice(0, 1024)).astype(BF16)
-        send(("ry1", jj), s1y.at[jj], ry1.at[jj], y_peer)
-
-    def stage2(jj):
-        got(("rx1", jj), rx1.at[jj])
-        s2y[jj] = (both(jj, 0, 0, near) + rx1[jj, 0].astype(F32)).astype(BF16)
-        send(("ry2", jj), s2y.at[jj], ry2.at[jj], y_peer)
-        got(("ry1", jj), ry1.at[jj])
-        s2x[jj] = (both(jj, 1, 1, far) + ry1[jj, far, :].astype(F32)).astype(BF16)
-        send(("rx2", jj), s2x.at[jj], rx2.at[jj], x_peer)
-
-    def stage3(jj, o):
-        if o == 0:
-            got(("ry2", jj), ry2.at[jj])
+        part = slice(i * 256, (i + 1) * 256)
+        for n in range(2):
+            base = pl.multiple_of((ysel[yr] * 2 + cc) * 512 + n * 256, 256)
+            cs = pl.ds(base, 256)
+            v = dot(tokh[part, 0:width], wd[0, :, cs]) + dot(tokh[part, width : 2 * width], wd[1, :, cs])
+            if d == 0:
+                v = jnp.concatenate([v[:rows], v[rows:] + dot(shh[...], sd[:, cs])], axis=0)
+            out[i, yr, :, n * 256 : (n + 1) * 256] = v.astype(BF16)
+        if peer:
+            send(("rc", i, yr), mo_peer.at[i, yr], rc.at[i, yr], c_peer)
+
+    def both(i, yr, part):
+        return mo_own[i, yr, part, :].astype(F32) + rc[i, yr, part, :].astype(F32)
+
+    far, near = slice(0, 128), slice(128, 256)
+
+    @scoped
+    def stage1(d, yr):
+        i = turn[d]
+        got(("rc", i, yr), rc.at[i, yr])
+        s1x[i, yr] = both(i, yr, far).astype(BF16)
+        send(("rx1", i, yr), s1x.at[i, yr], rx1.at[i, yr], x_peer)
+
+    @scoped
+    def stage2(d):
+        i = turn[d]
+        got(("rx1", i, 0), rx1.at[i, 0])
+        s2y[i] = (both(i, 0, near) + rx1[i, 0].astype(F32)).astype(BF16)
+        send(("ry2", i), s2y.at[i], ry2.at[i], y_peer)
+
+    @scoped
+    def stage3(d):
+        i = turn[d]
+        got(("rx1", i, 1), rx1.at[i, 1])
+        v = both(i, 1, near) + rx1[i, 1].astype(F32)
+        got(("ry2", i), ry2.at[i])
+        v = v + ry2[i].astype(F32)
+        if d:
+            s3[d - 1] = v.astype(BF16)
+            send(("rz", d), s3.at[d - 1], rz.at[d - 1], z_peer[d])
         else:
-            got(("rx2", jj), rx2.at[jj])
-        for d in (2, 3, 1, 0):
-            part = slice(512 + d * 128, 512 + (d + 1) * 128)
-            here = slice(d * 128, (d + 1) * 128)
-            v = both(jj, 1, o, part)
-            if o == 0:
-                v = v + rx1[jj, 1, here, :].astype(F32) + ry2[jj, here, :].astype(F32)
-            else:
-                v = v + ry1[jj, part, :].astype(F32) + rx2[jj, here, :].astype(F32)
-            if d:
-                s3[jj, o, d - 1] = v.astype(BF16)
-                send(("rz", jj, o, d), s3.at[jj, o, d - 1], rz.at[jj, o, d - 1], z_peer[d])
-            else:
-                keep[jj, o] = v
-
-    def final(jj, o):
-        v = keep[jj, o]
-        for d in (1, 2, 3):
-            got(("rz", jj, o, d), rz.at[jj, o, d - 1])
-            v = v + rz[jj, o, d - 1].astype(F32)
-        at = jj * 256 + o * 128
-        moe_out[:, at : at + 128] = v.astype(BF16)
+            keep[...] = v
+
+    @scoped
+    def final():
+        v = keep[...]
+        for d in (2, 3, 1):
+            got(("rz", d), rz.at[d - 1])
+            v = v + rz[d - 1].astype(F32)
+        moe_out[...] = v.astype(BF16)
+
+    @scoped
+    def mixer_sum():
+        got(("mrc", 0), mrc.at[0])
+        ms[...] = (mp[ysel[0] * 2 + c].astype(F32) + mrc[0].astype(F32)).astype(BF16)
+
+    def mixer_send():
+        send("mry", ms, mry, y_peer)
+
+    @scoped
+    def mixer_final():
+        got(("mrc", 1), mrc.at[1])
+        got("mry", mry)
+        mix_out[...] = (
+            mp[ysel[1] * 2 + c].astype(F32) + mrc[1].astype(F32) + mry[...].astype(F32)
+        ).astype(BF16)
+
+    @scoped
+    def halo_in():
+        @pl.when(me == 0)
+        def _():
+            halo_r[...] = jnp.zeros_like(halo_r)
+
+        @pl.when(me > 0)
+        def _():
+            got("halo", halo_r)
+
+        store_kv(halo_r[:, 0:128].astype(F32), halo_r[:, 128:256].astype(F32), 0)
 
     need("ag", "tf", "fine", "coarse")
     qkv(3)
@@ -402,104 +452,118 @@
     def _():
         copy("halo", halo_s, halo_r, {"ep": (me + 1) % n_ep, "tp": t}).start()
 
-    arrived("z", R(1, 1), 1)
-    to_x(1)
-    to_core(R(1, 1), 1)
-    arrived("x", R(0, 0), 1)
-    to_core(R(0, 0), 1)
+    def cores(d):
+        for r in pair(d):
+            if r != own:
+                from_core(r)
+
     qkv(0)
     qkv(1)
-    arrived("z", R(2, 1), 1)
-    to_x(2)
-    to_y(R(2, 1))
-    to_core(R(2, 1), 1)
-    arrived("x", R(0, 0), 0)
-    to_core(R(0, 0), 0)
+    arrive("x", 0, 0, 1, 0)
+    arrive("x", 0, 0, 1, 1)
     qkv(2)
+    arrive("z", 2, 1, 1, 0, "y", "x")
+    arrive("x", 0, 0, 0, 0)
     onehots()
-    arrived("z", R(3, 1), 1)
-    to_x(3)
-    to_y(R(3, 1))
-    to_core(R(3, 1), 1)
-    arrived("z", R(1, 1), 0)
-    to_core(R(1, 1), 0)
+    arrive("x", 0, 0, 0, 1)
     attend(1)
-    arrived("x", R(1, 0), 1)
-    to_y(R(1, 0))
-    to_core(R(1, 0), 1)
+    arrive("z", 2, 1, 1, 1, "y", "x")
+    shared_hidden()
     attend(2)
-    arrived("x", R(2, 0), 1)
-    to_y(R(2, 0))
-    to_core(R(2, 0), 1)
+    arrive("y", 2, 1, 0, 0)
+    arrive("x", 2, 0, 1, 0, "y")
+    cores(0)
+    dispatch(0)
+    gate_up(0, 0)
+    arrive("z", 3, 1, 1, 0, "x", "y")
+    arrive("y", 2, 1, 0, 1)
+    gate_up(0, 1)
+    to_tokens(0)
+    arrive("x", 2, 0, 1, 1, "y")
+    down(0, 0, True)
+    down(0, 1, True)
+    arrive("y", 2, 0, 0, 0)
+    arrive("z", 1, 1, 1, 0, "x")
+    arrive("z", 3, 1, 1, 1, "x", "y")
+    down(0, 0, False)
+    down(0, 1, False)
     attend(3)
-
-    @pl.when(me == 0)
-    def _():
-        halo_r[...] = jnp.zeros_like(halo_r)
-
-    @pl.when(me > 0)
-    def _():
-        got("halo", halo_r)
-
-    store_kv(halo_r[:, 0:128].astype(F32), halo_r[:, 128:256].astype(F32), 0)
+    arrive("z", 1, 1, 0, 0, "x")
+    arrive("x", 3, 0, 1, 0, "y")
+    arrive("y", 3, 1, 0, 0)
+    halo_in()
     attend(0)
-    arrived("x", R(3, 0), 1)
-    to_y(R(3, 0))
-    to_core(R(3, 0), 1)
     for k in (0, 1):
         send(("mrc", k), mp.at[ysel[k] * 2 + 1 - c], mrc.at[k], c_peer)
-    shared_hidden()
-    from_y(R(2, 1))
-    from_y(R(3, 1))
-    got(("mrc", 0), mrc.at[0])
-    ms[...] = (mp[ysel[0] * 2 + c].astype(F32) + mrc[0].astype(F32)).astype(BF16)
-    send("mry", ms, mry, y_peer)
-    from_y(R(1, 0))
-    first = (R(0, 1), R(0, 0), R(1, 1), R(1, 0))
-    second = (R(2, 1), R(3, 1), R(2, 0), R(3, 0))
-    for r in first[1:]:
-        from_core(r)
-    dispatch(0, first)
-    gate_up(0, first, 0)
-    from_y(R(2, 0))
-    gate_up(0, first, 1)
-    from_y(R(3, 0))
-    to_tokens(first)
-    for r in second:
-        from_core(r)
-    dispatch(1, second)
-    gate_up(1, second, 0)
-    gate_up(1, second, 1)
-    to_tokens(second)
-    for jj in range(2):
-        for yr in range(2):
-            down(jj, yr, mo_peer, 1 - c)
-        core_send(jj)
-        for yr in range(2):
-            down(jj, yr, mo_own, c)
-        stage1(jj)
+    arrive("y", 2, 0, 0, 1)
+    arrive("z", 1, 1, 1, 1, "x")
+    mixer_sum()
+    cores(2)
+    dispatch(2)
+    arrive("z", 1, 1, 0, 1, "x")
+    stage1(0, 1)
+    arrive("x", 3, 0, 1, 1, "y")
+    mixer_send()
+    arrive("y", 3, 1, 0, 1)
+    gate_up(2, 0)
+    arrive("x", 1, 0, 1, 0)
+    arrive("x", 1, 0, 0, 0)
+    arrive("y", 3, 0, 0, 0)
+    gate_up(2, 1)
+    arrive("x", 1, 0, 1, 1)
+    to_tokens(2)
+    down(2, 0, True)
+    down(2, 1, True)
+    arrive("x", 1, 0, 0, 1)
+    arrive("y", 3, 0, 0, 1)
+    down(2, 0, False)
+    stage1(2, 0)
+    down(2, 1, False)
+    stage1(2, 1)
+    cores(3)
+    dispatch(3)
+    gate_up(3, 0)
+    gate_up(3, 1)
+    to_tokens(3)
+    down(3, 0, True)
+    down(3, 1, True)
+    down(3, 0, False)
+    stage1(3, 0)
+    down(3, 1, False)
+    stage1(3, 1)
+    stage2(2)
+    cores(1)
+    dispatch(1)
+    gate_up(1, 0)
+    gate_up(1, 1)
+    to_tokens(1)
+    down(1, 0, True)
+    down(1, 1, True)
+    down(1, 0, False)
+    stage1(1, 0)
+    stage1(0, 0)
+    down(1, 1, False)
+    stage1(1, 1)
+    stage2(3)
+    stage3(2)
+    stage2(1)
     stage2(0)
-    got(("mrc", 1), mrc.at[1])
-    got("mry", mry)
-    mix_out[...] = (
-        mp[ysel[1] * 2 + c].astype(F32) + mrc[1].astype(F32) + mry[...].astype(F32)
-    ).astype(BF16)
-    stage3(0, 0)
-    stage3(0, 1)
-    stage2(1)
-    final(0, 0)
-    final(0, 1)
-    stage3(1, 0)
-    stage3(1, 1)
-    final(1, 0)
-    final(1, 1)
+    stage3(3)
+    mixer_final()
+    stage3(1)
+    stage3(0)
+    final()
 
     @pl.when(me < n_ep - 1)
     def _():
         copy("halo", halo_s, halo_r, {"ep": (me + 1) % n_ep, "tp": t}).wait_send()
 
-    for k in started:
-        k.wait_send()
+    @scoped
+    def all_sent():
+        for k in started:
+            k.wait_send()
+
+    all_sent()
     assert not loads and len(ids) <= ss.shape[0]
 
 
@@ -524,11 +588,13 @@
         sink, ag.reshape(1, -1), fg.reshape(1, -1), routes.T, rweight.T, fine, coarse,
         tf, wq, wk, wv, wo, ts, wg, wu, wd, sg, su, sd,
     )
+    args = tuple(pltpu.with_memory_space_constraint(a, pltpu.HBM) for a in args)
     vm = pl.BlockSpec(memory_space=pltpu.VMEM)
-    hbm = pl.BlockSpec(memory_space=pl.ANY)
+    hbm = pl.BlockSpec(memory_space=pltpu.HBM)
     v = pltpu.VMEM
     dma = pltpu.SemaphoreType.DMA
     qw = wide // 4
+    two = 2 * rows
     scratch = [v(a.shape, a.dtype) for a in args[1:]] + [
         v((tf.shape[0], 256), BF16),
         v((2, tf.shape[0] + rows, 128), BF16),
@@ -540,7 +606,7 @@
         v((n_ep, exp_dev * cap, rows), BF16),
         v((n_ep, exp_dev, rows, exp_dev * cap), BF16),
         v((n_ep, exp_dev, cap, 1), F32),
-        v((exp_dev, n_ep * cap, wide), BF16),
+        v((exp_dev, 2 * cap, wide), BF16),
         v((n_ep * exp_dev * cap, hidden), BF16),
         v((n_ep * rows, exp_dev * hidden), BF16),
         v((rows, sg.shape[1]), BF16),
@@ -548,21 +614,17 @@
         v((2, mrows, wide), BF16),
         v((mrows, wide), BF16),
         v((mrows, wide), BF16),
-        v((2, 2, 2, n_ep * rows, 128), BF16),
-        v((2, 2, 2, n_ep * rows, 128), BF16),
-        v((2, 2, 2, n_ep * rows, 128), BF16),
-        v((2, 2, 4 * rows, 128), BF16),
-        v((2, 2, 4 * rows, 128), BF16),
-        v((2, 8 * rows, 128), BF16),
-        v((2, 8 * rows, 128), BF16),
-        v((2, 4 * rows, 128), BF16),
-        v((2, 4 * rows, 128), BF16),
-        v((2, 4 * rows, 128), BF16),
-        v((2, 4 * rows, 128), BF16),
-        v((2, 2, 3, rows, 128), BF16),
-        v((2, 2, 3, rows, 128), BF16),
-        v((2, 2, rows, 128), F32),
-        dma((18,)), dma((72,)), dma((72,)),
+        v((4, 2, two, qw), BF16),
+        v((4, 2, two, qw), BF16),
+        v((4, 2, two, qw), BF16),
+        v((4, 2, rows, qw), BF16),
+        v((4, 2, rows, qw), BF16),
+        v((4, rows, qw), BF16),
+        v((4, rows, qw), BF16),
+        v((3, rows, qw), BF16),
+        v((3, rows, qw), BF16),
+        v((rows, qw), F32),
+        dma((18,)), dma((120,)), dma((120,)),
     ]
     moe_out_shape = jax.ShapeDtypeStruct((rows, qw), BF16)
     mix_out_shape = jax.ShapeDtypeStruct((mrows, wide), BF16)
@@ -573,7 +635,7 @@
         out_specs=(vm, vm),
         scratch_shapes=scratch,
         compiler_params=pltpu.CompilerParams(
-            collective_id=0, has_side_effects=True, vmem_limit_bytes=60 * 1024 * 1024
+            collective_id=0, has_side_effects=True, vmem_limit_bytes=50 * 1024 * 1024
         ),
         name="fused",
     )(*args)

time: 78.1 us -> 64.4 us (0.82)
  Pallas kernels: 73.8 us -> 62.1 us
  local copies, waits for them, and re-layouts: 3.45 us -> 1.45 us
    pallas_call x1, Pallas kernels: 73.8 us -> 62.1 us  [fused(): pl.pallas_call(functools.partial(fused_kernel, cap), out_shape=(mix_out_s...]
    unnamed x2, local copies, waits for them, and re-layouts: 3.45 us -> 1.45 us
where the time goes in v2:
time: 64.4 us; the launch traced here: 64.2 us
  Pallas kernels  62.1 us (96%)
  local copies, waits for them, and re-layouts  1.45 us (2%)
  between operations  0.65 us (1%)
    pallas_call x1, Pallas kernels, fused(): pl.pallas_call(functools.partial(fused_kernel, cap), out_shape=(mix_out_s...  62.1 us
    unnamed x2, local copies, waits for them, and re-layouts  1.45 us

profile of v2, /device:TPU:0, one launch (start us, length us, event | category | flops | bytes accessed | tf_op | source)
XLA Modules:
  0.0 64.2 jit_solution(8532093458460758123)
XLA Ops:
  0.6 62.1 %fused.1 = (bf16[128,2048]{1,0:T(8,128)(2,1)S(1)}, bf16[128,512]{1,0:T(8,128)(2,1)S(1)}) custom-call(f32[4]{0:T(128)} %sinks.1, f32[1,2048]{1,0:T(1,128)} %bitcast.4, f32[1,2048]{1,0:T(1,128)} %bitcast.5, s32[4,128]{1,0:T(4,128)} %bitcast.6, f32[4,128]{1,0:T(4,128)} %bitcast.7, f32[2,128,128]{2,1,0:T(8,128)} %constant.4.clone.fine_h, ...), custom_call_target="tpu_custom_call" | custom-call | tf_op jit(solution)/shard_map/fused/pallas_call | solution.py:631
  62.8 0.8 %copy.23 = bf16[128,2048]{1,0:T(8,128)(2,1)} copy(bf16[128,2048]{1,0:T(8,128)(2,1)S(1)} %get-tuple-element.4) | data formatting | bytes 1048576
  63.6 0.7 %copy.24 = bf16[128,512]{1,0:T(8,128)(2,1)} copy(bf16[128,512]{1,0:T(8,128)(2,1)S(1)} %get-tuple-element.5) | data formatting | bytes 262144

commit v3 on v2

--- a/solution.py
+++ b/solution.py
@@ -68,7 +68,7 @@
     mix_out, moe_out,
     ag, fg, rt, rw, fine, coarse, tf, wq, wk, wv, wo, ts, wg, wu, wd, sg, su, sd,
     qs, kd, vd, halo_s, halo_r, xg, mg, oh, oht, wsl, xs, hid, tokh, shh,
-    mp, mrc, ms, mry, mo_own, mo_peer, rc, s1x, rx1, s2y, ry2, s3, rz, keep,
+    mp, mrc, ms, mry, mo_own, mo_peer, rc, s1x, rx1, s2y, ry2, s3, rz, s4, rl, keep,
     lsem, ss, rs,
 ):
     me, t = lax.axis_index("ep"), lax.axis_index("tp")
@@ -77,6 +77,7 @@
     z_peer = [{"ep": zd * 2 + x, "tp": t} for zd in zs]
     x_peer = {"ep": z * 2 + 1 - x, "tp": t}
     y_peer = {"ep": me, "tp": (1 - y) * 2 + c}
+    zy_peer = {"ep": zs[1] * 2 + x, "tp": (1 - y) * 2 + c}
     c_peer = {"ep": me, "tp": y * 2 + 1 - c}
     n_ep = 8
     exp_dev = wg.shape[0]
@@ -113,23 +114,34 @@
         pl.semaphore_signal(
             barrier, inc=1, device_id={"ep": (me + e) % n_ep, "tp": t}, device_id_type=MESH
         )
-    for peer in (y_peer, c_peer):
+    for peer in (y_peer, c_peer, zy_peer):
         pl.semaphore_signal(barrier, inc=1, device_id=peer, device_id_type=MESH)
 
     ids = {}
     started = []
 
+    together = {"m": mg.at[0 : n_ep - 1], "rc": rc, "rx1": rx1}
+    for way in "xyzc":
+        together[way] = xg.at[0 : n_ep - 1]
+    groups = {}
+
     def copy(name, src, dst, peer):
         i = ids.setdefault(name, len(ids))
+        kind = name[0] if isinstance(name, tuple) else name
+        kind = "x" if kind in "xyzc" else kind
+        key = kind if kind in together else name
+        j = groups.setdefault(key, len(groups))
         return pltpu.make_async_remote_copy(
-            src_ref=src, dst_ref=dst, send_sem=ss.at[i], recv_sem=rs.at[i],
+            src_ref=src, dst_ref=dst, send_sem=ss.at[j], recv_sem=rs.at[i],
             device_id=peer, device_id_type=MESH,
         )
 
     def send(name, src, dst, peer):
         k = copy(name, src, dst, peer)
         k.start()
-        started.append(k)
+        kind = name[0] if isinstance(name, tuple) else name
+        if kind not in together:
+            started.append(k)
 
     def got(name, dst):
         copy(name, dst, dst, c_peer).wait_recv()
@@ -150,28 +162,6 @@
     def q_of(k, cc):
         return (y if k else 1 - y) * 2 + cc
 
-    @scoped
-    def norm_second():
-        need("ts", "fg", "rt", "rw")
-        xn = normed(ts[...].astype(F32), fg[...])
-        for q in range(4):
-            xg[own, q] = xn[:, q * quarter : (q + 1) * quarter]
-        mg[own] = jnp.concatenate([rt[...].astype(F32), rw[...]], axis=0)
-
-    norm_second()
-
-    @scoped
-    def barrier_wait():
-        pl.semaphore_wait(barrier, n_ep + 1)
-
-    barrier_wait()
-
-    for s in (0, 1):
-        for d in range(4):
-            if R(d, s) != own:
-                peer = {"ep": zs[d] * 2 + (x if s else 1 - x), "tp": t}
-                send(("m", R(d, s)), mg.at[own], mg.at[R(d, s)], peer)
-
     parts = 2
     sub = rows // parts
 
@@ -182,15 +172,39 @@
         q = q_of(k, c)
         send((link, at, k, p), piece(own, q, p), piece(at, q, p), peer)
 
+    @scoped
+    def norm_second(p):
+        part = slice(p * sub, (p + 1) * sub)
+        xn = normed(ts[part].astype(F32), fg[...])
+        for q in range(4):
+            xg[own, q, part] = xn[:, q * quarter : (q + 1) * quarter]
+
+    @scoped
+    def barrier_wait():
+        pl.semaphore_wait(barrier, n_ep + 2)
+
+    need("ts", "fg", "rt", "rw")
+    mg[own] = jnp.concatenate([rt[...].astype(F32), rw[...]], axis=0)
     for p in range(parts):
+        norm_second(p)
+        if p == 0:
+            barrier_wait()
+            for s in (0, 1):
+                for d in range(4):
+                    if R(d, s) != own:
+                        peer = {"ep": zs[d] * 2 + (x if s else 1 - x), "tp": t}
+                        send(("m", R(d, s)), mg.at[own], mg.at[R(d, s)], peer)
         block_send("z", 1, z_peer[2], R(2, 1), p)
         block_send("x", 1, x_peer, R(0, 0), p)
-    for p in range(parts):
-        block_send("z", 1, z_peer[3], R(3, 1), p)
-        block_send("x", 0, x_peer, R(0, 0), p)
-    for p in range(parts):
-        block_send("z", 1, z_peer[1], R(1, 1), p)
-        block_send("z", 0, z_peer[1], R(1, 1), p)
+
+    def send_three():
+        for p in range(parts):
+            block_send("z", 1, z_peer[3], R(3, 1), p)
+
+    def send_one():
+        for p in range(parts):
+            block_send("z", 1, z_peer[1], R(1, 1), p)
+            block_send("z", 0, z_peer[1], R(1, 1), p)
 
     def arrive(link, d, s, k, p, *onward):
         at, q = R(d, s), q_of(k, c)
@@ -377,58 +391,80 @@
         if peer:
             send(("rc", i, yr), mo_peer.at[i, yr], rc.at[i, yr], c_peer)
 
-    def both(i, yr, part):
-        return mo_own[i, yr, part, :].astype(F32) + rc[i, yr, part, :].astype(F32)
+    def span(h):
+        return pl.ds(0, 512) if h is None else pl.ds(h * 256, 256)
+
+    def both(i, yr, part, h=None):
+        at = span(h)
+        return mo_own[i, yr, part, at].astype(F32) + rc[i, yr, part, at].astype(F32)
 
     far, near = slice(0, 128), slice(128, 256)
 
     @scoped
-    def stage1(d, yr):
-        i = turn[d]
-        got(("rc", i, yr), rc.at[i, yr])
-        s1x[i, yr] = both(i, yr, far).astype(BF16)
-        send(("rx1", i, yr), s1x.at[i, yr], rx1.at[i, yr], x_peer)
+    def stage1(d, yr, h=None):
+        i, at = turn[d], span(h)
+        if not h:
+            got(("rc", i, yr), rc.at[i, yr])
+        s1x[i, yr, :, at] = both(i, yr, far, h).astype(BF16)
+        send(("rx1", i, yr, h), s1x.at[i, yr, :, at], rx1.at[i, yr, :, at], x_peer)
 
     @scoped
     def stage2(d):
         i = turn[d]
-        got(("rx1", i, 0), rx1.at[i, 0])
+        got(("rx1", i, 0, None), rx1.at[i, 0])
         s2y[i] = (both(i, 0, near) + rx1[i, 0].astype(F32)).astype(BF16)
         send(("ry2", i), s2y.at[i], ry2.at[i], y_peer)
 
     @scoped
+    def last(yr, h):
+        i, at = turn[1], span(h)
+        got(("rx1", i, yr, h), rx1.at[i, yr, :, at])
+        s4[yr, :, at] = (both(i, yr, near, h) + rx1[i, yr, :, at].astype(F32)).astype(BF16)
+        send(("rl", yr, h), s4.at[yr, :, at], rl.at[yr, :, at], z_peer[1] if yr else zy_peer)
+
+    @scoped
     def stage3(d):
         i = turn[d]
-        got(("rx1", i, 1), rx1.at[i, 1])
+        got(("rx1", i, 1, None), rx1.at[i, 1])
         v = both(i, 1, near) + rx1[i, 1].astype(F32)
         got(("ry2", i), ry2.at[i])
         v = v + ry2[i].astype(F32)
         if d:
-            s3[d - 1] = v.astype(BF16)
-            send(("rz", d), s3.at[d - 1], rz.at[d - 1], z_peer[d])
+            s3[d - 2] = v.astype(BF16)
+            send(("rz", d), s3.at[d - 2], rz.at[d - 2], z_peer[d])
         else:
             keep[...] = v
 
     @scoped
     def final():
         v = keep[...]
-        for d in (2, 3, 1):
-            got(("rz", d), rz.at[d - 1])
-            v = v + rz[d - 1].astype(F32)
-        moe_out[...] = v.astype(BF16)
+        for d in (2, 3):
+            got(("rz", d), rz.at[d - 2])
+            v = v + rz[d - 2].astype(F32)
+        for h in range(2):
+            at = span(h)
+            u = v[:, h * 256 : (h + 1) * 256]
+            for yr in range(2):
+                got(("rl", yr, h), rl.at[yr, :, at])
+                u = u + rl[yr, :, at].astype(F32)
+            moe_out[:, at] = u.astype(BF16)
 
     @scoped
     def mixer_sum():
         got(("mrc", 0), mrc.at[0])
         ms[...] = (mp[ysel[0] * 2 + c].astype(F32) + mrc[0].astype(F32)).astype(BF16)
 
-    def mixer_send():
-        send("mry", ms, mry, y_peer)
+    def mixer_rows(i):
+        return pl.ds(i * (rows // 4), rows // 4)
+
+    def mixer_send(i):
+        send(("mry", i), ms.at[mixer_rows(i)], mry.at[mixer_rows(i)], y_peer)
 
     @scoped
     def mixer_final():
         got(("mrc", 1), mrc.at[1])
-        got("mry", mry)
+        for i in range(4):
+            got(("mry", i), mry.at[mixer_rows(i)])
         mix_out[...] = (
             mp[ysel[1] * 2 + c].astype(F32) + mrc[1].astype(F32) + mry[...].astype(F32)
         ).astype(BF16)
@@ -459,71 +495,77 @@
 
     qkv(0)
     qkv(1)
-    arrive("x", 0, 0, 1, 0)
-    arrive("x", 0, 0, 1, 1)
+    arrive("x", 0, 0, 1, 0, "y")
+    arrive("x", 0, 0, 1, 1, "y")
     qkv(2)
+    send_three()
+    attend(1)
     arrive("z", 2, 1, 1, 0, "y", "x")
-    arrive("x", 0, 0, 0, 0)
     onehots()
-    arrive("x", 0, 0, 0, 1)
-    attend(1)
+    attend(2)
+    arrive("y", 0, 0, 0, 0)
     arrive("z", 2, 1, 1, 1, "y", "x")
     shared_hidden()
-    attend(2)
+    send_one()
+    attend(3)
+    arrive("y", 0, 0, 0, 1)
     arrive("y", 2, 1, 0, 0)
+    halo_in()
+    attend(0)
+    for k in (0, 1):
+        send(("mrc", k), mp.at[ysel[k] * 2 + 1 - c], mrc.at[k], c_peer)
     arrive("x", 2, 0, 1, 0, "y")
     cores(0)
     dispatch(0)
     gate_up(0, 0)
+    arrive("y", 2, 1, 0, 1)
     arrive("z", 3, 1, 1, 0, "x", "y")
-    arrive("y", 2, 1, 0, 1)
     gate_up(0, 1)
     to_tokens(0)
     arrive("x", 2, 0, 1, 1, "y")
     down(0, 0, True)
-    down(0, 1, True)
     arrive("y", 2, 0, 0, 0)
     arrive("z", 1, 1, 1, 0, "x")
+    down(0, 1, True)
     arrive("z", 3, 1, 1, 1, "x", "y")
     down(0, 0, False)
+    arrive("z", 1, 1, 0, 0, "x")
+    stage1(0, 0)
     down(0, 1, False)
-    attend(3)
-    arrive("z", 1, 1, 0, 0, "x")
     arrive("x", 3, 0, 1, 0, "y")
+    arrive("y", 2, 0, 0, 1)
     arrive("y", 3, 1, 0, 0)
-    halo_in()
-    attend(0)
-    for k in (0, 1):
-        send(("mrc", k), mp.at[ysel[k] * 2 + 1 - c], mrc.at[k], c_peer)
-    arrive("y", 2, 0, 0, 1)
     arrive("z", 1, 1, 1, 1, "x")
-    mixer_sum()
     cores(2)
     dispatch(2)
     arrive("z", 1, 1, 0, 1, "x")
     stage1(0, 1)
+    gate_up(2, 0)
+    gate_up(2, 1)
+    to_tokens(2)
     arrive("x", 3, 0, 1, 1, "y")
-    mixer_send()
-    arrive("y", 3, 1, 0, 1)
-    gate_up(2, 0)
-    arrive("x", 1, 0, 1, 0)
-    arrive("x", 1, 0, 0, 0)
-    arrive("y", 3, 0, 0, 0)
-    gate_up(2, 1)
-    arrive("x", 1, 0, 1, 1)
-    to_tokens(2)
+    mixer_sum()
+    mixer_send(0)
+    mixer_send(1)
     down(2, 0, True)
     down(2, 1, True)
-    arrive("x", 1, 0, 0, 1)
-    arrive("y", 3, 0, 0, 1)
+    arrive("y", 3, 1, 0, 1)
+    arrive("y", 3, 0, 0, 0)
     down(2, 0, False)
     stage1(2, 0)
     down(2, 1, False)
     stage1(2, 1)
+    arrive("y", 3, 0, 0, 1)
+    stage2(0)
+    mixer_send(2)
     cores(3)
     dispatch(3)
+    arrive("x", 1, 0, 1, 0)
+    arrive("x", 1, 0, 0, 0)
     gate_up(3, 0)
+    arrive("x", 1, 0, 1, 1)
     gate_up(3, 1)
+    arrive("x", 1, 0, 0, 1)
     to_tokens(3)
     down(3, 0, True)
     down(3, 1, True)
@@ -531,27 +573,30 @@
     stage1(3, 0)
     down(3, 1, False)
     stage1(3, 1)
-    stage2(2)
     cores(1)
     dispatch(1)
+    stage2(2)
     gate_up(1, 0)
     gate_up(1, 1)
     to_tokens(1)
     down(1, 0, True)
     down(1, 1, True)
+    stage2(3)
+    mixer_send(3)
     down(1, 0, False)
-    stage1(1, 0)
-    stage1(0, 0)
+    stage1(1, 0, 0)
+    stage1(1, 0, 1)
+    stage3(2)
     down(1, 1, False)
-    stage1(1, 1)
-    stage2(3)
-    stage3(2)
-    stage2(1)
-    stage2(0)
+    stage1(1, 1, 0)
+    stage1(1, 1, 1)
     stage3(3)
+    last(0, 0)
+    last(0, 1)
+    last(1, 0)
+    last(1, 1)
+    stage3(0)
     mixer_final()
-    stage3(1)
-    stage3(0)
     final()
 
     @pl.when(me < n_ep - 1)
@@ -562,9 +607,15 @@
     def all_sent():
         for k in started:
             k.wait_send()
+        for kind in ("x", "m", "rc", "rx1"):
+            whole, sem = together[kind], ss.at[groups[kind]]
+            pltpu.make_async_remote_copy(
+                src_ref=whole, dst_ref=whole, send_sem=sem, recv_sem=sem,
+                device_id=c_peer, device_id_type=MESH,
+            ).wait_send()
 
     all_sent()
-    assert not loads and len(ids) <= ss.shape[0]
+    assert not loads and (len(ids), len(groups)) == (rs.shape[0], ss.shape[0]), (len(ids), len(groups))
 
 
 def rope_tables(tokens, rows):
@@ -621,10 +672,12 @@
         v((4, 2, rows, qw), BF16),
         v((4, rows, qw), BF16),
         v((4, rows, qw), BF16),
-        v((3, rows, qw), BF16),
-        v((3, rows, qw), BF16),
+        v((2, rows, qw), BF16),
+        v((2, rows, qw), BF16),
+        v((2, rows, qw), BF16),
+        v((2, rows, qw), BF16),
         v((rows, qw), F32),
-        dma((18,)), dma((120,)), dma((120,)),
+        dma((18,)), dma((20,)), dma((97,)),
     ]
     moe_out_shape = jax.ShapeDtypeStruct((rows, qw), BF16)
     mix_out_shape = jax.ShapeDtypeStruct((mrows, wide), BF16)

time: 64.4 us -> 62.9 us (0.977)
  Pallas kernels: 62.1 us -> 60.7 us
    pallas_call x1, Pallas kernels: 62.1 us -> 60.7 us  [fused(): pl.pallas_call(functools.partial(fused_kernel, cap), out_shape=(mix_out_s...]
where the time goes in v3:
time: 62.9 us; the launch traced here: 62.8 us
  Pallas kernels  60.7 us (97%)
  local copies, waits for them, and re-layouts  1.45 us (2%)
  between operations  0.65 us (1%)
    pallas_call x1, Pallas kernels, fused(): pl.pallas_call(functools.partial(fused_kernel, cap), out_shape=(mix_out_s...  60.7 us
    unnamed x2, local copies, waits for them, and re-layouts  1.45 us

profile of v3, /device:TPU:0, one launch (start us, length us, event | category | flops | bytes accessed | tf_op | source)
XLA Modules:
  0.0 62.8 jit_solution(4532566655308257588)
XLA Ops:
  0.6 60.7 %fused.1 = (bf16[128,2048]{1,0:T(8,128)(2,1)S(1)}, bf16[128,512]{1,0:T(8,128)(2,1)S(1)}) custom-call(f32[4]{0:T(128)} %sinks.1, f32[1,2048]{1,0:T(1,128)} %bitcast.4, f32[1,2048]{1,0:T(1,128)} %bitcast.5, s32[4,128]{1,0:T(4,128)} %bitcast.6, f32[4,128]{1,0:T(4,128)} %bitcast.7, f32[2,128,128]{2,1,0:T(8,128)} %constant.4.clone.fine_h, ...), custom_call_target="tpu_custom_call" | custom-call | tf_op jit(solution)/shard_map/fused/pallas_call | solution.py:684
  61.3 0.8 %copy.23 = bf16[128,2048]{1,0:T(8,128)(2,1)} copy(bf16[128,2048]{1,0:T(8,128)(2,1)S(1)} %get-tuple-element.4) | data formatting | bytes 1048576
  62.1 0.7 %copy.24 = bf16[128,512]{1,0:T(8,128)(2,1)} copy(bf16[128,512]{1,0:T(8,128)(2,1)S(1)} %get-tuple-element.5) | data formatting | bytes 262144
